TPU v7x, 512 devices: a whole 4x8x8 slice. The times are simulated.
512 devices in a mesh: sp: 32 (over z, x), tp: 16 (over y, core).
Axes of the slice: x: 4, y: 8, z: 8, core: 2. Of those that a mesh axis runs over, the one named last changes fastest.
Arguments:
- stream_in: bfloat16 [8192, 2048], P(('sp', 'tp')), may hold values from -6 to 6
- queries: bfloat16 [8192, 4096], P('sp', 'tp'), may hold values from -6 to 6
- key_rows: bfloat16 [8192, 4096], P('sp', 'tp'), may hold values from -6 to 6
- values: bfloat16 [8192, 8192], P('sp', 'tp'), may hold values from -6 to 6
- decay_low: bfloat16 [8192, 16], P('sp'), may hold values from -4 to 4
- decay_matrix: bfloat16 [16, 4096], P(None, 'tp'), may hold values from -1.5 to 1.5
- decay_bias: float32 [4096], P('tp')
- decay_shift: float32 [8192, 16], P('sp', 'tp'), may hold values from -1 to 0
- head_gain: float32 [512], replicated, may hold values from 0.1 to 1.9
- output_matrix: bfloat16 [8192, 2048], P('tp'), may hold values from -0.0625 to 0.0625
- feed_gain: float32 [2048], replicated, may hold values from 0.1 to 1.9
- routes: int32 [8192, 2], P('sp'), may hold values from 0 to 31, all different within a row; in each aligned block of 256 rows (0 to 255, 256 to 511, ...) at most 16 rows name the same one
- route_weights: float32 [8192, 2], P('sp'), may hold values from 0.2 to 1
- expert_gate: bfloat16 [32, 2048, 2816], P('sp', None, 'tp'), may hold values from -0.125 to 0.125
- specialist_widen: bfloat16 [32, 2048, 2816], P('sp', None, 'tp'), may hold values from -0.125 to 0.125
- expert_down: bfloat16 [32, 2816, 2048], P('sp', 'tp'), may hold values from -0.109375 to 0.109375
Outputs:
- layer_out: bfloat16 [8192, 2048], P(('sp', 'tp'))
Inputs may be any that keep to these rules, and one draw needn't show every extreme that they name: `routes`: each row names 2 different experts; within each aligned block of 256 rows no expert is named by more than 16 rows, and in every draw some expert is named by exactly 16 rows of some block.
All inputs are finite; a program needn't handle non-finite values.
Results may differ from a plain program's by a relative error of at most 0.02.
Values may be sent and summed in bfloat16 or wider, within the bound.
A program may use at most 64 MiB of HBM per device.

v0:
```python
import jax
import jax.numpy as jnp
from jax import lax
from jax.sharding import Mesh
from jax.sharding import PartitionSpec as P

HK = 256
HV = 512
TOP = 2
BLK = 128
SP = ("sp_0", "sp_1")
TP = ("tp_0", "tp_1")
SP_TP = ("sp_0", "sp_1", "tp_0", "tp_1")


TEMPER = 16.0
EPSILON = 1e-06
HIGHEST = lax.Precision.HIGHEST


def filled_with(shard, identity):
    return jax.tree.map(
        lambda part, zero: jnp.zeros_like(part) + jnp.asarray(zero, part.dtype), shard, identity
    )


def carried_in(shard, axes, combine, identity):
    before = start = filled_with(shard, identity)
    so_far = shard
    for axis in reversed(axes):
        peers, here = (lax.axis_size(axis), lax.axis_index(axis))
        pieces = jax.tree.map(
            lambda part, kind: lax.all_gather(part.astype(kind), axis),
            so_far,
            (jnp.bfloat16, jnp.bfloat16),
        )
        inside, so_far = (start, start)
        for k in range(peers):
            passed = k < here
            so_far = combine(
                so_far, jax.tree.map(lambda part, own: part[k].astype(own.dtype), pieces, shard)
            )
            inside = jax.tree.map(lambda new, old: jnp.where(passed, new, old), so_far, inside)
        before = combine(inside, before)
    return before


def cut_along(shard, dim, peers):
    before, after = (shard.shape[:dim], shard.shape[dim + 1 :])
    return jnp.moveaxis(shard.reshape(*before, peers, -1, *after), dim, 0)


def sent_and_summed(shard, axis, dim):
    tiles = cut_along(shard, dim, lax.axis_size(axis))
    arrived = lax.all_to_all(tiles, axis, split_axis=0, concat_axis=0, tiled=True)
    return arrived.astype(jnp.float32).sum(axis=0)


def gathered_by_axis(shard, axes, dim):
    for axis in reversed(axes):
        shard = lax.all_gather(shard, axis, axis=dim, tiled=True)
    return shard


def decay_logs(decay_low, decay_matrix, decay_bias, decay_shift, heads):
    before_gate = jnp.dot(decay_low, decay_matrix, preferred_element_type=jnp.float32) + decay_bias
    logged = jax.nn.log_sigmoid(before_gate) / TEMPER
    return logged.reshape(before_gate.shape[0], heads, HK) + decay_shift[:, :, None]


def into_blocks(array):
    length, heads, width = array.shape
    return array.reshape(length // BLK, BLK, heads, width).transpose(2, 0, 1, 3)


def segment_summands(queries, key_rows, values, log_decay):
    inside = jnp.cumsum(log_decay, axis=2)
    final_position = inside[:, :, -1:, :]
    scaled_query = queries * jnp.exp(inside) * HK ** (-0.5)
    scaled_key = key_rows * jnp.exp(-inside)
    end_keys = key_rows * jnp.exp(final_position - inside)
    scores = jnp.einsum("hnid,hnjd->hnij", scaled_query, scaled_key, precision=HIGHEST)
    causal = jnp.tril(jnp.ones((BLK, BLK), jnp.bool_))
    scores = jnp.where(causal, scores, 0.0)
    local_out = jnp.einsum("hnij,hnjv->hniv", scores, values, precision=HIGHEST)
    partial_update = jnp.einsum("hnjd,hnjv->hndv", end_keys, values, precision=HIGHEST)
    return (scaled_query, local_out, partial_update, jnp.exp(final_position[:, :, 0, :]))


def run_blocks(scaled_query, partial_update, block_decay, start):

    def advance(state, pieces):
        query_block, added, decay = pieces
        output = jnp.einsum("hid,hdv->hiv", query_block, state, precision=HIGHEST)
        return (state * decay[:, :, None] + added, output)

    final, outputs = lax.scan(
        advance,
        start,
        (
            jnp.moveaxis(scaled_query, 1, 0),
            jnp.moveaxis(partial_update, 1, 0),
            jnp.moveaxis(block_decay, 1, 0),
        ),
    )
    return (final, jnp.moveaxis(outputs, 0, 1))


def link_states(earlier, later):
    return (earlier[0] * later[0], earlier[1] * later[0][..., None] + later[1])


def pass_state(device_decay, local_state):
    identity = (jnp.ones_like(device_decay), jnp.zeros_like(local_state))
    _, carried = carried_in((device_decay, local_state), SP, link_states, identity)
    return carried


def head_norm(heads_out, head_gain):
    heads = heads_out.shape[0]
    flat = heads_out.transpose(1, 2, 0, 3).reshape(-1, heads, HV)
    normed = flat * lax.rsqrt(jnp.mean(flat * flat, axis=-1, keepdims=True) + EPSILON) * head_gain
    return normed.reshape(-1, heads * HV).astype(jnp.bfloat16)


def root_scale(midstream, gain):
    return (
        midstream
        * lax.rsqrt(jnp.mean(midstream * midstream, axis=-1, keepdims=True) + EPSILON)
        * gain
    ).astype(jnp.bfloat16)


def body(
    stream_in,
    queries,
    key_rows,
    values,
    decay_low,
    decay_matrix,
    decay_bias,
    decay_shift,
    head_gain,
    output_matrix,
    feed_gain,
    routes,
    route_weights,
    expert_gate,
    specialist_widen,
    expert_down,
):
    length = queries.shape[0]
    heads = queries.shape[1] // HK
    sequence_devices = lax.axis_size(SP)
    head_devices = lax.axis_size(TP)
    width = stream_in.shape[1]
    log_decay = decay_logs(decay_low, decay_matrix, decay_bias, decay_shift, heads)

    def shaped(array, channels):
        return into_blocks(array.astype(jnp.float32).reshape(length, heads, channels))

    scaled_query, local_out, partial_update, block_decay = segment_summands(
        shaped(queries, HK), shaped(key_rows, HK), shaped(values, HV), into_blocks(log_decay)
    )
    start = jnp.zeros((heads, HK, HV), jnp.float32)
    device_decay = jnp.prod(block_decay, axis=1)
    local_state, carried_out = run_blocks(scaled_query, partial_update, block_decay, start)
    carried = pass_state(device_decay, local_state)
    shifted = jnp.concatenate([jnp.ones_like(block_decay[:, :1]), block_decay[:, :-1]], axis=1)
    before = jnp.cumprod(shifted, axis=1)
    readout = jnp.einsum(
        "hnid,hdv->hniv", scaled_query * before[:, :, None, :], carried, precision=HIGHEST
    )
    total_out = local_out + carried_out + readout
    mixed = head_norm(total_out, head_gain)
    rows_here = length // head_devices
    attended = sent_and_summed(
        jnp.dot(mixed, output_matrix, preferred_element_type=jnp.float32).astype(jnp.bfloat16),
        TP,
        0,
    )
    midstream = stream_in.astype(jnp.float32) + attended
    normed = root_scale(midstream, feed_gain)
    group = lax.all_gather(normed, TP, axis=0, tiled=True)
    experts = sequence_devices * expert_gate.shape[0]
    capacity = head_devices * max(1, TOP * length // (sequence_devices * head_devices))
    block_slots = capacity // head_devices
    own_index = lax.axis_index(TP)
    flat_routes = routes.reshape(-1)
    expert_index = jnp.arange(experts, dtype=jnp.int32)
    matches = (flat_routes[:, None] == expert_index[None, :]).astype(jnp.int32)
    ranking = jnp.sum((jnp.cumsum(matches, axis=0) - matches) * matches, axis=1)
    slot_member = (ranking[:, None] - 0 == jnp.arange(capacity, dtype=jnp.int32)[None, :]).astype(
        jnp.float32
    )
    table = slot_member[:, :, None] * matches[:, None, :].astype(jnp.float32)
    full_table = table.reshape(length, TOP, capacity * experts)
    selector = jnp.sum(full_table, axis=1).T.astype(jnp.bfloat16)
    filled = jnp.dot(selector, group, preferred_element_type=jnp.float32)
    arrived = lax.all_to_all(
        filled.astype(jnp.bfloat16).reshape(capacity, experts, width),
        SP,
        split_axis=1,
        concat_axis=1,
        tiled=True,
    )
    rows_in = arrived.reshape(-1, width)
    gated = jnp.dot(rows_in, expert_gate[0], preferred_element_type=jnp.float32)
    lifted = jnp.dot(rows_in, specialist_widen[0], preferred_element_type=jnp.float32)
    hidden = (jax.nn.silu(gated) * lifted).astype(jnp.bfloat16)
    summed = sent_and_summed(
        jnp.dot(hidden, expert_down[0], preferred_element_type=jnp.float32).astype(jnp.bfloat16),
        TP,
        0,
    )
    expert_token_rows = summed.astype(jnp.bfloat16).reshape(block_slots, sequence_devices, width)
    returned = lax.all_to_all(expert_token_rows, SP, split_axis=1, concat_axis=1, tiled=True)
    weight_table = jnp.sum(full_table * route_weights.reshape(length, TOP, 1), axis=1)
    own_weights = lax.dynamic_slice_in_dim(weight_table, own_index * rows_here, rows_here, 0)
    piece = gathered_by_axis(returned, TP, 0)
    count = piece.shape[0]
    flat_piece = piece.reshape(count * experts, width).astype(jnp.float32)
    routed = jnp.dot(own_weights, flat_piece, precision=HIGHEST, preferred_element_type=jnp.float32)
    return (midstream + routed).astype(jnp.bfloat16)


def solution(mesh):
    finer = Mesh(mesh.devices.reshape(8, 4, 8, 2), ("sp_0", "sp_1", "tp_0", "tp_1"))
    in_specs = (
        P(SP_TP, None),
        P(SP, TP),
        P(SP, TP),
        P(SP, TP),
        P(SP, None),
        P(None, TP),
        P(TP),
        P(SP, TP),
        P(),
        P(TP, None),
        P(),
        P(SP, None),
        P(SP, None),
        P(SP, None, TP),
        P(SP, None, TP),
        P(SP, TP, None),
    )
    out_specs = P(SP_TP, None)
    return jax.shard_map(body, mesh=finer, in_specs=in_specs, out_specs=out_specs, check_vma=False)
```

profile of v0, /device:TPU:1, one launch (start us, length us, event | category | flops | bytes accessed | tf_op | source)
XLA Modules:
  0.0 366.4 jit_solution(5884363078821731961)
XLA Ops:
  6.5 1.3 fusion.71
  9.1 2.6 convolution_bitcast_fusion.1
  11.7 4.6 %while.13 = (s32[]{:T(128)}, f32[1,256,512]{2,1,0:T(8,128)S(1)}, f32[2,1,128,512]{3,2,1,0:T(8,128)}, f32[2,1,256]{2,1,0:T(1,128)S(1)}, f32[2,1,256,512]{3,2,1,0:...) while((s32[]{:T(128)}, f32[1,256,512]{2,1,0:T(8,128)S(1)}, ...), condition=%wide.region_2.3_spmd.clone, body=%wide.region_1.2_spmd.clone.sunk | while | flops 201850880 | bytes 2494568 | solution.py:97
  11.7 1.2 fusion.144
  12.8 1.2 bitcast_add_fusion.2
  15.1 1.2 bitcast_add_fusion.2
  17.2 8.5 %all-gather.2 = bf16[4,1,256]{2,1,0:T(2,128)(2,1)S(1)} all-gather(bf16[1,1,256]{2,1,0:T(2,128)(2,1)S(1)} %reshape.1207), channel_id=2, replica_groups=mesh['sp_0'=8,'sp_1'=4,'tp_0'=8,'tp_1'=2] {'sp_1'}, dimensions={0}, use_global_device_ids=true | all-gather | bytes 2560 | tf_op jit(solution)/shard_map/all_gather | solution.py:33
  25.7 24.4 %all-gather.14.cloned.1.call-done = bf16[4,256,512]{2,1,0:T(8,128)(2,1)} async-done(((bf16[1,256,512]{2,1,0:T(8,128)(2,1)}), bf16[4,256,512]{2,1,0:T(8,128)(2,1)}) %all-gather.14.cloned.1.call-update) | async-done | bytes 1048592 | tf_op jit(solution)/shard_map/all_gather | solution.py:33
  50.1 2.2 fusion.25
  52.5 13.5 %all_gather.28 = bf16[8,1,256]{2,1,0:T(2,128)(2,1)S(1)} all-gather(bf16[1,1,256]{2,1,0:T(2,128)(2,1)S(1)} %reshape.1214), channel_id=1, replica_groups=mesh['sp_0'=8,'sp_1'=4,'tp_0'=8,'tp_1'=2] {'sp_0'}, dimensions={0}, use_global_device_ids=true | all-gather | bytes 4608 | tf_op jit(solution)/shard_map/all_gather | solution.py:33
  66.5 28.3 %all-gather.8.cloned.1.call-done = bf16[8,1,256,512]{3,2,1,0:T(8,128)(2,1)} async-done(((bf16[1,1,256,512]{3,2,1,0:T(8,128)(2,1)}), bf16[8,1,256,512]{3,2,1,0:T(8,128)(2,1)}) %all-gather.8.cloned.1.call-update) | async-done | bytes 2097168 | tf_op jit(solution)/shard_map/all_gather | solution.py:33
  94.8 3.5 fusion.35
  99.7 39.9 %all_to_all.20 = bf16[16,16,2048]{2,1,0:T(8,128)(2,1)S(1)} all-to-all(bf16[16,16,2048]{2,1,0:T(8,128)(2,1)S(1)} %bitcast.272), channel_id=1, replica_groups=mesh['sp_0'=8,'sp_1'=4,'tp_0'=8,'tp_1'=2] {'tp_0','tp_1'}, dimensions={0} | all-to-all | bytes 2097152 | tf_op jit(solution)/shard_map/all_to_all | solution.py:55
  141.4 1.2 reduce-window.9
  143.2 4.1 %broadcast_multiply_fusion = f32[512,16,32]{2,1,0:T(8,128)} fusion(f32[512,32]{1,0:T(8,128)S(1)} %copy.45, f32[512,16]{1,0:T(8,128)S(1)} %fusion.96), kind=kLoop, calls=%fused_computation.17 | loop fusion | flops 262144 | bytes 1146880 | tf_op jit(solution)/shard_map/mul | solution.py:196
  147.3 3.9 %mul.567 = f32[256,2,512]{2,1,0:T(2,128)S(1)} reshape(f32[512,16,32]{2,1,0:T(8,128)} %broadcast_multiply_fusion) | data formatting | bytes 2097152 | tf_op jit(solution)/shard_map/mul | solution.py:196
  151.9 4.2 %multiply_reduce_fusion = (f32[256,512]{1,0:T(8,128)}, bf16[256,512]{1,0:T(8,128)(2,1)S(1)}) fusion(f32[256,2,512]{2,1,0:T(2,128)S(1)} %mul.567, f32[256,2]{1,0:T(8,128)} %copy.46), kind=kLoop, calls=%fused_computation.27 | loop fusion | flops 524288 | bytes 1837056 | tf_op jit(solution)/shard_map/reduce_sum | solution.py:218
  156.1 19.7 %all-gather.10.cloned.1.call-done = bf16[256,2048]{1,0:T(8,128)(2,1)} async-done(((bf16[16,2048]{1,0:T(8,128)(2,1)}), bf16[256,2048]{1,0:T(8,128)(2,1)}) %all-gather.10.cloned.1.call-update) | async-done | bytes 1048592 | tf_op jit(solution)/shard_map/all_gather | solution.py:184
  175.8 2.0 convolution_convert_fusion.1
  177.7 1.2 copy.47
  178.9 59.0 %all_to_all.21 = bf16[16,32,2048]{2,0,1:T(8,128)(2,1)S(1)} all-to-all(bf16[16,32,2048]{2,0,1:T(8,128)(2,1)S(1)} %copy.47), channel_id=1, replica_groups=mesh['sp_0'=8,'sp_1'=4,'tp_0'=8,'tp_1'=2] {'sp_0','sp_1'}, dimensions={1} | all-to-all | bytes 4194304 | tf_op jit(solution)/shard_map/all_to_all | solution.py:200
  237.9 1.2 copy.48
  239.0 1.3 copy-done.1
  240.3 1.6 fusion.16
  241.9 4.8 %convolution_convert_fusion = bf16[512,2048]{1,0:T(8,128)(2,1)} fusion(bf16[512,2048]{1,0:T(8,128)(2,1)} %bitcast.277, bf16[1,176,2048]{2,1,0:T(8,128)(2,1)S(1)} %copy-done.13, bf16[1,2048,176]{1,2,0:T(8,128)(2,1)} %param.32, f32[512,176]{0,1:T(8,128)} %fusion.16), kind=kOutput, calls=%fused_computation.12 | convolution fusion | flops 739786752 | bytes 5996544 | tf_op jit(solution)/shard_map/dot_general | solution.py:212
  246.7 57.8 %all_to_all.22 = bf16[16,32,2048]{2,1,0:T(8,128)(2,1)} all-to-all(bf16[16,32,2048]{2,1,0:T(8,128)(2,1)} %bitcast.278), channel_id=1, replica_groups=mesh['sp_0'=8,'sp_1'=4,'tp_0'=8,'tp_1'=2] {'tp_0','tp_1'}, dimensions={0} | all-to-all | bytes 4194304 | tf_op jit(solution)/shard_map/all_to_all | solution.py:55
  304.5 2.0 reduce_sum.72
  307.2 1.4 reduce.8
  308.7 15.5 %all_to_all.23 = bf16[32,2,1024]{2,1,0:T(2,128)(2,1)S(1)} all-to-all(bf16[32,2,1024]{2,1,0:T(2,128)(2,1)S(1)} %reshape.1223), channel_id=1, replica_groups=mesh['sp_0'=8,'sp_1'=4,'tp_0'=8,'tp_1'=2] {'sp_0','sp_1'}, dimensions={0} | all-to-all | bytes 262144 | tf_op jit(solution)/shard_map/all_to_all | solution.py:217
  324.4 2.1 all_gather.33
  326.5 30.2 %all-gather.12.cloned.1.call-done = bf16[16,32,2048]{2,1,0:T(8,128)(2,1)} async-done(((bf16[2,32,2048]{2,1,0:T(8,128)(2,1)}), bf16[16,32,2048]{2,1,0:T(8,128)(2,1)}) %all-gather.12.cloned.1.call-update) | async-done | bytes 2097168 | tf_op jit(solution)/shard_map/all_gather | solution.py:61
  356.7 3.2 fusion.9
  (84 shorter events, 9.4 us)
Async XLA Ops:
  6.5 92.4 %copy-start = (bf16[512,2048]{1,0:T(8,128)(2,1)S(1)}, bf16[512,2048]{1,0:T(8,128)(2,1)}, u32[]{:S(2)}) copy-start(bf16[512,2048]{1,0:T(8,128)(2,1)} %param.27) | copy-start | bytes 6291460
  6.5 2.5 copy-start.7
  6.5 43.5 %all-gather.14.cloned.1.call-start = ((), (), s32[]{:S(2)}) async-start(), calls=%async_computation.7 | async-start | bytes 1310720 | tf_op jit(solution)/shard_map/all_gather | solution.py:33
  16.3 36.1 %copy-start.6 = (bf16[256,256]{1,0:T(8,128)(2,1)S(1)}, bf16[256,256]{1,0:T(8,128)(2,1)}, u32[]{:S(2)}) copy-start(bf16[256,256]{1,0:T(8,128)(2,1)} %param.19) | copy-start | bytes 393220
  17.1 77.7 %all-gather.8.cloned.1.call-start = ((), (), s32[]{:S(2)}) async-start(), calls=%async_computation.4 | async-start | bytes 2359296 | tf_op jit(solution)/shard_map/all_gather | solution.py:33
  52.2 123.5 %all-gather.10.cloned.1.call-start = ((), (), s32[]{:S(2)}) async-start(), calls=%async_computation.5 | async-start | bytes 1114112 | tf_op jit(solution)/shard_map/all_gather | solution.py:184
  94.8 3.5 copy-start.2
  94.8 3.5 copy-start.5
  94.8 4.0 %copy-start.9 = (f32[512]{0:T(512)S(1)}, f32[512]{0:T(512)}, u32[]{:S(2)}) copy-start(f32[512]{0:T(512)} %param.26) | copy-start | bytes 6148
  99.7 40.1 %copy-start.3 = (bf16[16,2048]{1,0:T(8,128)(2,1)S(1)}, bf16[16,2048]{1,0:T(8,128)(2,1)}, u32[]{:S(2)}) copy-start(bf16[16,2048]{1,0:T(8,128)(2,1)} %param.18) | copy-start | bytes 196612
  99.7 40.2 %copy-start.8 = (f32[2048]{0:T(1024)S(1)}, f32[2048]{0:T(1024)}, u32[]{:S(2)}) copy-start(f32[2048]{0:T(1024)} %param.28) | copy-start | bytes 24580
  99.7 41.2 %copy-start.10 = (s32[256,2]{0,1:T(2,128)S(1)}, s32[256,2]{0,1:T(2,128)}, u32[]{:S(2)}) copy-start(s32[256,2]{0,1:T(2,128)} %param.29) | copy-start | bytes 6148
  140.7 216.0 %all-gather.12.cloned.1.call-start = ((), (), s32[]{:S(2)}) async-start(), calls=%async_computation.6 | async-start | bytes 2359296 | tf_op jit(solution)/shard_map/all_gather | solution.py:61
  147.3 3.9 %copy-start.11 = (f32[256,2]{0,1:T(2,128)S(1)}, f32[256,2]{0,1:T(2,128)}, u32[]{:S(2)}) copy-start(f32[256,2]{0,1:T(2,128)} %param.30) | copy-start | bytes 6148
  237.9 2.5 copy-start.12
  239.0 1.3 copy-start.1
  240.3 1.6 copy-start.13
  304.5 52.2 %copy-start.4 = (bf16[16,2048]{1,0:T(8,128)(2,1)S(1)}, bf16[16,2048]{1,0:T(8,128)(2,1)}, u32[]{:S(2)}) copy-start(bf16[16,2048]{1,0:T(8,128)(2,1)} %param.18) | copy-start | bytes 196612
Sparse Core Ops, SparseCore 0:
  17.2 32.8 all-gather.13
  52.4 42.3 all-gather.7
  140.8 34.9 all-gather.9
  326.6 30.0 all-gather.11
where the time goes:
time: 370 us; the launch traced here: 366 us
  blocking collectives  196 us (53%)
  waiting for transfers between devices  103 us (28%)
  matrix products  22.8 us (6%)
  other arithmetic  20.8 us (6%)
  between operations  13.5 us (4%)
  local copies, waits for them, and re-layouts  10.1 us (3%)
    all_to_all x2, blocking collectives, sent_and_summed(): lax.all_to_all(tiles, axis, split_axis=0, concat_axis=0, tiled=True)  97.7 us
    all_to_all x1, blocking collectives, body(): lax.all_to_all(filled.astype(jnp.bfloat16).reshape(capacity, experts, wid...  59 us
    all_gather x2, waiting for transfers between devices, carried_in(): lax.all_gather(part.astype(kind), axis)  52.6 us
    all_gather x1, waiting for transfers between devices, gathered_by_axis(): shard = lax.all_gather(shard, axis, axis=dim, tiled=True)  30.2 us
    all_gather x2, blocking collectives, carried_in(): lax.all_gather(part.astype(kind), axis)  22 us
    all_gather x1, waiting for transfers between devices, body(): group = lax.all_gather(normed, TP, axis=0, tiled=True)  19.7 us
    all_to_all x1, blocking collectives, body(): lax.all_to_all(expert_token_rows, SP, split_axis=1, concat_axis=1, tiled=...  15.5 us
  transfers between devices with their start and end apart: 4, of which 4 were waited for; matrix products, arithmetic and copies ran while one was open for 4% of the time, Pallas kernels for 0%

commit v1 on v0

v1 whole, which is shorter than its diff:
```python
import functools

import jax
import jax.numpy as jnp
from jax import lax
from jax.experimental import pallas as pl
from jax.experimental.pallas import tpu as pltpu
from jax.sharding import PartitionSpec as P

BLK = 128
TEMPER = 16.0
EPSILON = 1e-06
PARTS = 4
BF = jnp.bfloat16
F32 = jnp.float32


def dot(a, b):
    return jnp.dot(a, b, preferred_element_type=F32)


def dot_nt(a, b):
    return lax.dot_general(a, b, (((1,), (1,)), ((), ())), preferred_element_type=F32)


def split2(x):
    high = x.astype(BF)
    return high, (x - high.astype(F32)).astype(BF)


def split3(x):
    high = x.astype(BF)
    rest = x - high.astype(F32)
    middle = rest.astype(BF)
    return high, middle, (rest - middle.astype(F32)).astype(BF)


def remote(src, dst, send_sem, recv_sem, device):
    return pltpu.make_async_remote_copy(
        src_ref=src,
        dst_ref=dst,
        send_sem=send_sem,
        recv_sem=recv_sem,
        device_id=device,
        device_id_type=pl.DeviceIdType.MESH,
    )


def iota(shape, dim):
    return lax.broadcasted_iota(jnp.int32, shape, dim)


def layer_kernel(
    size,
    stream,
    queries,
    key_rows,
    values,
    decay_low,
    decay_matrix,
    decay_bias,
    decay_shift,
    head_gain,
    w_any,
    feed_gain,
    routes,
    route_weights,
    gate_any,
    up_any,
    down_any,
    out,
    w_s,
    gate_s,
    up_s,
    down_s,
    query_s,
    total_s,
    update_s,
    state_send,
    state_recv,
    prior_send,
    prior_recv,
    select_s,
    weight_high,
    weight_low,
    mixed_s,
    pair_send,
    pair_recv,
    own_s,
    row_send,
    row_recv,
    mid_s,
    norm_send,
    norm_recv,
    slot_send,
    rows_s,
    gate_acc,
    up_acc,
    hidden_s,
    half_send,
    half_recv,
    half_own,
    sum_send,
    sum_recv,
    back_send,
    back_recv,
    last_send,
    last_recv,
    load_sem,
    state_ss,
    state_rs,
    prior_ss,
    prior_rs,
    pair_ss,
    pair_rs,
    row_ss,
    row_rs,
    norm_ss,
    norm_rs,
    slot_ss,
    slot_rs,
    ring_ss,
    ring_rs,
    mate_ss,
    mate_rs,
    half_ss,
    half_rs,
    sum_ss,
    sum_rs,
    back_ss,
    back_rs,
    last_ss,
    last_rs,
):
    n_sp, n_tp, rows, width, piece = size
    n_y = n_tp // 2
    half_ring = n_y // 2
    length = rows * n_tp
    slots = 2 * length // n_sp
    columns = width // n_tp
    part_width = width // PARTS
    hk = queries.shape[1]
    hv = values.shape[1]
    sp = lax.axis_index("sp")
    tp = lax.axis_index("tp")
    y = lax.div(tp, 2)
    core = lax.rem(tp, 2)
    other = 1 - core
    mate = (sp, tp + 1 - 2 * core)

    loads = []
    for i, (src, dst) in enumerate(
        (
            (w_any, w_s),
            (gate_any.at[0], gate_s),
            (up_any.at[0], up_s),
            (down_any.at[0], down_s.at[pl.ds(0, piece)]),
        )
    ):
        loads.append(pltpu.make_async_copy(src, dst, load_sem.at[i]))
        loads[-1].start()

    barrier = pltpu.get_barrier_semaphore()

    def greet_sp(i, carry):
        pl.semaphore_signal(
            barrier,
            inc=1,
            device_id=(lax.rem(sp + i, n_sp), tp),
            device_id_type=pl.DeviceIdType.MESH,
        )
        return carry

    def greet_tp(i, carry):
        pl.semaphore_signal(
            barrier,
            inc=1,
            device_id=(sp, lax.rem(tp + i, n_tp)),
            device_id_type=pl.DeviceIdType.MESH,
        )
        return carry

    lax.fori_loop(1, n_sp, greet_sp, 0)
    lax.fori_loop(1, n_tp, greet_tp, 0)

    before_gate = dot(decay_low[...], decay_matrix[...]) + decay_bias[...]
    logs = (
        jnp.minimum(before_gate, 0.0) - jnp.log1p(jnp.exp(-jnp.abs(before_gate)))
    ) / TEMPER + decay_shift[...]
    lower = iota((BLK, BLK), 0) >= iota((BLK, BLK), 1)
    lower_ones = jnp.where(lower, 1.0, 0.0).astype(BF)
    inside = []
    finals = []
    final_columns = []
    scaled_keys = []
    for n in range(2):
        block = slice(n * BLK, (n + 1) * BLK)
        high, middle, low = split3(logs[block])
        summed = dot(lower_ones, high) + (dot(lower_ones, middle) + dot(lower_ones, low))
        final = summed[BLK - 1 : BLK, :]
        keys = key_rows[block, :].astype(F32)
        end_keys = keys * jnp.exp(final - summed)
        high, low = split2(end_keys.T)
        update = dot(high, values[block, :]) + dot(low, values[block, :])
        update_s[n] = update
        inside.append(summed)
        finals.append(jnp.exp(final))
        final_columns.append(jnp.exp(jnp.broadcast_to(final, (BLK, hk)).T))
        scaled_keys.append(keys * jnp.exp(-summed))
    whole_decay = final_columns[0] * final_columns[1]
    for m in range(hv // BLK):
        lanes = slice(m * BLK, (m + 1) * BLK)
        state = update_s[0, :, lanes] * final_columns[1] + update_s[1, :, lanes]
        state_send[:, :, lanes] = state.reshape(n_sp, hk // n_sp, BLK).astype(BF)
    high, low = split2(whole_decay)
    packed = jnp.where(
        iota((hk, BLK), 1) < BLK // 2, high.astype(F32), low.astype(F32)
    )
    state_send[:, :, hv : hv + BLK] = packed.reshape(n_sp, hk // n_sp, BLK).astype(BF)

    pl.semaphore_wait(barrier, n_sp - 1 + n_tp - 1)

    def send_state(i, carry):
        peer = lax.rem(sp + i, n_sp)
        remote(
            state_send.at[peer], state_recv.at[sp], state_ss, state_rs.at[sp], (peer, tp)
        ).start()
        return carry

    lax.fori_loop(1, n_sp, send_state, 0)
    state_recv[sp] = state_send[sp]

    for n in range(2):
        block = slice(n * BLK, (n + 1) * BLK)
        query = queries[block, :].astype(F32) * jnp.exp(inside[n]) * hk**-0.5
        query_high, query_low = split2(query)
        key_high, key_low = split2(scaled_keys[n])
        scores = dot_nt(query_high, key_high) + (
            dot_nt(query_high, key_low) + dot_nt(query_low, key_high)
        )
        scores = jnp.where(lower, scores, 0.0)
        high, low = split2(scores)
        total = dot(high, values[block, :]) + dot(low, values[block, :])
        if n == 1:
            high, low = split2(update_s[0])
            total += dot(query_high, high) + (dot(query_high, low) + dot(query_low, high))
            query = query * finals[0]
        total_s[block, :] = total
        query_s[block, :] = query

    expert = iota((length, n_sp), 1)
    first = jnp.where(routes[:, 0:1] == expert, 1.0, 0.0)
    second = jnp.where(routes[:, 1:2] == expert, 1.0, 0.0)
    named = first + second
    earlier = jnp.where(iota((length, length), 0) > iota((length, length), 1), 1.0, 0.0)
    rank = dot(earlier.astype(BF), named.astype(BF))
    place = (named * (rank + 1.0)).astype(BF)
    count = n_sp * slots
    start = iota((count, n_sp), 1) * slots
    at = iota((count, n_sp), 0)
    spread = jnp.where((at >= start) & (at < start + slots), 1.0, 0.0).astype(BF)
    slot = ((iota((count, length), 0) & (slots - 1)) + 1).astype(F32)
    select_s[...] = jnp.where(dot_nt(spread, place) == slot, 1.0, 0.0).astype(BF)
    start = iota((n_sp, count), 0) * slots
    at = iota((n_sp, count), 1)
    spread = jnp.where((at >= start) & (at < start + slots), 1.0, 0.0).astype(BF)
    slot = ((iota((length, count), 1) & (slots - 1)) + 1).astype(F32)
    chosen = dot(place, spread) == slot
    high, low = split2(first * route_weights[:, 0:1] + second * route_weights[:, 1:2])
    weight_high[...] = jnp.where(chosen, dot(high, spread), 0.0).astype(BF)
    weight_low[...] = jnp.where(chosen, dot(low, spread), 0.0).astype(BF)

    for n in range(PARTS):
        row_recv[n, y] = jnp.zeros(row_recv.shape[2:], BF)
    down_s[piece:, :] = jnp.zeros((down_s.shape[0] - piece, width), BF)
    hidden_s[...] = jnp.zeros(hidden_s.shape, BF)

    def carry_state(j, state):
        prior_send[j] = state.astype(BF)

        @pl.when(j != sp)
        def _():
            remote(
                state_send.at[j], state_recv.at[j], state_ss, state_rs.at[j], (j, tp)
            ).wait_recv()
            remote(
                prior_send.at[j], prior_recv.at[sp], prior_ss, prior_rs, (j, tp)
            ).start()

        @pl.when(j == sp)
        def _():
            prior_recv[j] = state.astype(BF)

        came = state_recv[j].astype(F32)
        decay = came[:, hv : hv + 1] + came[:, hv + BLK // 2 : hv + BLK // 2 + 1]
        return state * decay + came[:, :hv]

    lax.fori_loop(0, n_sp, carry_state, jnp.zeros((hk // n_sp, hv), F32))
    most = pl.ds(0, n_sp - 1)
    remote(
        prior_send.at[most], prior_recv.at[most], prior_ss, prior_rs, mate
    ).wait_recv()
    carried = prior_recv[...].astype(F32).reshape(hk, hv).astype(BF)
    high, low = split2(query_s[...])
    total = total_s[...] + (dot(high, carried) + dot(low, carried))
    mixed = (
        total
        * lax.rsqrt(jnp.mean(total * total, axis=-1, keepdims=True) + EPSILON)
        * head_gain[...]
    ).astype(BF)
    mixed_s[...] = mixed.reshape(n_y, 2, rows, hv)

    def order(i):
        return jnp.where(
            lax.rem(i, 2) == 0, half_ring + lax.div(i, 2), half_ring - lax.div(i + 1, 2)
        )

    def pair_copy(n):
        return remote(
            pair_send.at[n], pair_recv.at[n], pair_ss.at[n], pair_rs.at[n], mate
        )

    def add_pair(n):
        pair_copy(n).wait_recv()
        total = own_s[n] + pair_recv[n].astype(F32)
        own_s[n] = total
        row_send[n] = total.astype(BF)

        def send_row(i, carry):
            yy = lax.rem(y + order(i), n_y)
            remote(
                row_send.at[n, yy],
                row_recv.at[n, y],
                row_ss.at[n],
                row_rs.at[n],
                (sp, 2 * yy + core),
            ).start()
            return carry

        lax.fori_loop(0, n_y - 1, send_row, 0)

    loads[0].wait()

    def project(n, carry):
        lanes = pl.ds(pl.multiple_of(n * part_width, part_width), part_width)
        theirs = mixed_s[:, other].reshape(n_y * rows, hv)
        pair_send[n] = dot(theirs, w_s[:, lanes]).astype(BF).reshape(n_y, rows, part_width)
        pair_copy(n).start()
        mine = mixed_s[:, core].reshape(n_y * rows, hv)
        product = dot(mine, w_s[:, lanes]).astype(BF).astype(F32)
        own_s[n] = product.reshape(n_y, rows, part_width)

        @pl.when(n > 0)
        def _():
            add_pair(n - 1)

        return carry

    lax.fori_loop(0, PARTS, project, 0)
    add_pair(PARTS - 1)

    rest = pl.ds(0, n_y - 1)
    for n in range(PARTS):
        lanes = slice(n * part_width, (n + 1) * part_width)
        remote(
            row_send.at[n, rest], row_recv.at[n, rest], row_ss.at[n], row_rs.at[n], mate
        ).wait_recv()
        total = own_s[n, y] + jnp.sum(row_recv[n].astype(F32), axis=0)
        mid_s[:, lanes] = stream[:, lanes].astype(F32) + total
    middle = mid_s[...]
    normed = (
        middle
        * lax.rsqrt(jnp.mean(middle * middle, axis=-1, keepdims=True) + EPSILON)
        * feed_gain[...]
    ).astype(BF)
    for j in range(n_tp):
        norm_send[j] = normed[:, j * columns : (j + 1) * columns]

    def to_tp(send, recv, send_sem, recv_sem):
        def start(i, carry):
            peer = lax.rem(tp + i, n_tp)
            remote(send.at[peer], recv.at[tp], send_sem, recv_sem, (sp, peer)).start()
            return carry

        lax.fori_loop(1, n_tp, start, 0)
        recv[tp] = send[tp]
        others = pl.ds(0, n_tp - 1)
        return remote(send.at[others], recv.at[others], send_sem, recv_sem, mate)

    norm_all = to_tp(norm_send, norm_recv, norm_ss, norm_rs)
    norm_all.wait_recv()
    group = norm_recv[...].reshape(length, columns)
    slot_send[...] = dot(select_s[...], group).astype(BF).reshape(n_sp, slots, columns)

    def send_slots(i, carry):
        peer = lax.rem(sp + i, n_sp)
        remote(
            slot_send.at[peer],
            rows_s.at[y, core, sp],
            slot_ss,
            slot_rs.at[sp],
            (peer, tp),
        ).start()
        return carry

    lax.fori_loop(1, n_sp, send_slots, 0)
    rows_s[y, core, sp] = slot_send[sp]

    n_half = n_sp // 2

    def ring_copy(d, step, p):
        yy = lax.rem(y + n_y + (1 - 2 * d) * (1 - step), n_y)
        to = lax.rem(y + n_y + 1 - 2 * d, n_y)
        part = rows_s.at[yy, core, pl.ds(p * n_half, n_half)]
        return remote(
            part, part, ring_ss.at[d, step, p], ring_rs.at[d, step, p], (sp, 2 * to + core)
        )

    def mate_copy(yy, c, p):
        part = rows_s.at[yy, c, pl.ds(p * n_half, n_half)]
        return remote(part, part, mate_ss.at[yy, p], mate_rs.at[yy, p], mate)

    for p in range(2):

        def wait_slots(b, carry):
            @pl.when(b != sp)
            def _():
                remote(
                    slot_send.at[b], rows_s.at[y, core, b], slot_ss, slot_rs.at[b], mate
                ).wait_recv()

            return carry

        lax.fori_loop(p * n_half, (p + 1) * n_half, wait_slots, 0)
        for d in range(2):
            if half_ring > 1 or d == p:
                ring_copy(d, 1, p).start()
        mate_copy(y, core, p).start()

    def pass_on(step):
        for p in range(2):
            for d in range(2):

                def one():
                    yy = lax.rem(y + n_y - (1 - 2 * d) * step, n_y)
                    ring_copy(d, step, p).wait_recv()
                    if d == p:
                        more = step < half_ring
                    else:
                        more = step + 1 < half_ring

                    @pl.when(more)
                    def _():
                        ring_copy(d, step + 1, p).start()

                    mate_copy(yy, core, p).start()

                if d == p:
                    one()
                else:
                    pl.when(step < half_ring)(one)

    loads[1].wait()
    loads[2].wait()
    loads[3].wait()
    gate_acc[...] = jnp.zeros(gate_acc.shape, F32)
    up_acc[...] = jnp.zeros(up_acc.shape, F32)

    def widen(m, carry):
        step = lax.div(m + 1, 2) + 1

        @pl.when(((m == 0) | (lax.rem(m, 2) == 1)) & (step <= half_ring))
        def _():
            pass_on(step)

        offset = jnp.where(lax.rem(m, 2) == 1, -lax.div(m + 1, 2), lax.div(m, 2))
        yy = lax.rem(y + n_y + offset, n_y)
        for p in range(2):
            mate_copy(yy, other, p).wait_recv()
        x = jnp.concatenate(
            [rows_s[yy, 0].reshape(count, columns), rows_s[yy, 1].reshape(count, columns)],
            axis=1,
        )
        depth = pl.ds(pl.multiple_of(yy * 2 * columns, 2 * columns), 2 * columns)
        gate_acc[...] += dot(x, gate_s[depth, :])
        up_acc[...] += dot(x, up_s[depth, :])
        return carry

    lax.fori_loop(0, n_y, widen, 0)
    gated = gate_acc[...]
    hidden = gated / (1.0 + jnp.exp(-gated)) * up_acc[...]
    hidden_s[:, 0:piece] = hidden.astype(BF)

    def half_copy(i):
        return remote(
            half_send.at[i], half_recv.at[i], half_ss.at[i], half_rs.at[i], mate
        )

    def add_half(i):
        yy = lax.rem(y + order(i), n_y)
        half_copy(i).wait_recv()
        total = half_own[i] + half_recv[i].astype(F32)
        half_own[i] = total

        @pl.when(i < n_y - 1)
        def _():
            sum_send[i] = total.astype(BF)
            remote(
                sum_send.at[i], sum_recv.at[y], sum_ss, sum_rs, (sp, 2 * yy + core)
            ).start()

    def lower_rows(i, carry):
        yy = lax.rem(y + order(i), n_y)
        lanes = pl.ds(pl.multiple_of(yy * 2 * columns, 2 * columns), 2 * columns)
        product = dot(hidden_s[...], down_s[:, lanes])
        left, right = product[:, :columns], product[:, columns:]
        half_send[i] = jnp.where(core == 0, right, left).astype(BF)
        half_copy(i).start()
        half_own[i] = jnp.where(core == 0, left, right).astype(BF).astype(F32)

        @pl.when(i > 0)
        def _():
            add_half(i - 1)

        return carry

    lax.fori_loop(0, n_y, lower_rows, 0)
    sum_recv[y] = jnp.zeros(sum_recv.shape[1:], BF)
    add_half(n_y - 1)
    remote(sum_send, sum_recv.at[rest], sum_ss, sum_rs, mate).wait_recv()
    total = half_own[n_y - 1] + jnp.sum(sum_recv[...].astype(F32), axis=0)
    back_send[...] = total.astype(BF).reshape(n_sp, slots, columns)

    def send_back(i, carry):
        peer = lax.rem(sp + i, n_sp)
        remote(back_send.at[peer], back_recv.at[sp], back_ss, back_rs, (peer, tp)).start()
        return carry

    lax.fori_loop(1, n_sp, send_back, 0)
    back_recv[sp] = back_send[sp]
    remote(back_send.at[most], back_recv.at[most], back_ss, back_rs, mate).wait_recv()
    returned = back_recv[...].reshape(count, columns)
    routed = dot(weight_high[...], returned) + dot(weight_low[...], returned)
    last_send[...] = routed.astype(BF).reshape(n_tp, rows, columns)
    last_all = to_tp(last_send, last_recv, last_ss, last_rs)
    last_all.wait_recv()
    for j in range(n_tp):
        lanes = slice(j * columns, (j + 1) * columns)
        out[:, lanes] = (mid_s[:, lanes] + last_recv[j].astype(F32)).astype(BF)

    remote(
        state_send.at[most], state_recv.at[most], state_ss, state_rs.at[0], mate
    ).wait_send()
    remote(prior_send.at[most], prior_recv.at[most], prior_ss, prior_rs, mate).wait_send()
    for n in range(PARTS):
        pair_copy(n).wait_send()
        remote(
            row_send.at[n, rest], row_recv.at[n, rest], row_ss.at[n], row_rs.at[n], mate
        ).wait_send()
    norm_all.wait_send()
    remote(
        slot_send.at[most], rows_s.at[0, 0, most], slot_ss, slot_rs.at[0], mate
    ).wait_send()
    for step in range(1, half_ring + 1):
        for d in range(2):
            for p in range(2):
                if step < half_ring or d == p:
                    ring_copy(d, step, p).wait_send()
    for yy in range(n_y):
        for p in range(2):
            mate_copy(yy, core, p).wait_send()
        half_copy(yy).wait_send()
    remote(sum_send, sum_recv.at[rest], sum_ss, sum_rs, mate).wait_send()
    remote(back_send.at[most], back_recv.at[most], back_ss, back_rs, mate).wait_send()
    last_all.wait_send()


def layer(
    n_sp,
    n_tp,
    stream_in,
    queries,
    key_rows,
    values,
    decay_low,
    decay_matrix,
    decay_bias,
    decay_shift,
    head_gain,
    output_matrix,
    feed_gain,
    routes,
    route_weights,
    expert_gate,
    specialist_widen,
    expert_down,
):
    rows, width = stream_in.shape
    length = queries.shape[0]
    hk, hv = queries.shape[1], values.shape[1]
    piece = expert_down.shape[1]
    n_y = n_tp // 2
    half_ring = n_y // 2
    slots = 2 * length // n_sp
    count = n_sp * slots
    columns = width // n_tp
    part = width // PARTS
    own = hk // n_sp
    padded = (piece + 127) // 128 * 128
    vmem, any_space = (
        pl.BlockSpec(memory_space=pltpu.VMEM),
        pl.BlockSpec(memory_space=pl.ANY),
    )
    dma = pltpu.SemaphoreType.DMA
    scratch = [
        pltpu.VMEM((hv, width), BF),
        pltpu.VMEM((width, piece), BF),
        pltpu.VMEM((width, piece), BF),
        pltpu.VMEM((padded, width), BF),
        pltpu.VMEM((length, hk), F32),
        pltpu.VMEM((length, hv), F32),
        pltpu.VMEM((2, hk, hv), F32),
        pltpu.VMEM((n_sp, own, hv + BLK), BF),
        pltpu.VMEM((n_sp, own, hv + BLK), BF),
        pltpu.VMEM((n_sp, own, hv), BF),
        pltpu.VMEM((n_sp, own, hv), BF),
        pltpu.VMEM((count, length), BF),
        pltpu.VMEM((length, count), BF),
        pltpu.VMEM((length, count), BF),
        pltpu.VMEM((n_y, 2, rows, hv), BF),
        pltpu.VMEM((PARTS, n_y, rows, part), BF),
        pltpu.VMEM((PARTS, n_y, rows, part), BF),
        pltpu.VMEM((PARTS, n_y, rows, part), F32),
        pltpu.VMEM((PARTS, n_y, rows, part), BF),
        pltpu.VMEM((PARTS, n_y, rows, part), BF),
        pltpu.VMEM((rows, width), F32),
        pltpu.VMEM((n_tp, rows, columns), BF),
        pltpu.VMEM((n_tp, rows, columns), BF),
        pltpu.VMEM((n_sp, slots, columns), BF),
        pltpu.VMEM((n_y, 2, n_sp, slots, columns), BF),
        pltpu.VMEM((count, piece), F32),
        pltpu.VMEM((count, piece), F32),
        pltpu.VMEM((count, padded), BF),
        pltpu.VMEM((n_y, count, columns), BF),
        pltpu.VMEM((n_y, count, columns), BF),
        pltpu.VMEM((n_y, count, columns), F32),
        pltpu.VMEM((n_y - 1, count, columns), BF),
        pltpu.VMEM((n_y, count, columns), BF),
        pltpu.VMEM((n_sp, slots, columns), BF),
        pltpu.VMEM((n_sp, slots, columns), BF),
        pltpu.VMEM((n_tp, rows, columns), BF),
        pltpu.VMEM((n_tp, rows, columns), BF),
        dma((4,)),
        dma,
        dma((n_sp,)),
        dma,
        dma,
        dma((PARTS,)),
        dma((PARTS,)),
        dma((PARTS,)),
        dma((PARTS,)),
        dma,
        dma,
        dma,
        dma((n_sp,)),
        dma((2, half_ring + 2, 2)),
        dma((2, half_ring + 2, 2)),
        dma((n_y, 2)),
        dma((n_y, 2)),
        dma((n_y,)),
        dma((n_y,)),
        dma,
        dma,
        dma,
        dma,
        dma,
        dma,
    ]
    return pl.pallas_call(
        functools.partial(layer_kernel, (n_sp, n_tp, rows, width, piece)),
        out_shape=jax.ShapeDtypeStruct((rows, width), BF),
        in_specs=[vmem] * 9 + [any_space] + [vmem] * 3 + [any_space] * 3,
        out_specs=vmem,
        scratch_shapes=scratch,
        compiler_params=pltpu.CompilerParams(
            collective_id=0, has_side_effects=True, vmem_limit_bytes=60 * 1024 * 1024
        ),
        name="layer",
    )(
        stream_in,
        queries,
        key_rows,
        values,
        decay_low,
        decay_matrix,
        decay_bias.reshape(1, -1),
        decay_shift,
        head_gain.reshape(1, -1),
        output_matrix,
        feed_gain.reshape(1, -1),
        routes,
        route_weights,
        expert_gate,
        specialist_widen,
        expert_down,
    )


def solution(mesh):
    in_specs = (
        P(("sp", "tp"), None),
        P("sp", "tp"),
        P("sp", "tp"),
        P("sp", "tp"),
        P("sp", None),
        P(None, "tp"),
        P("tp"),
        P("sp", "tp"),
        P(),
        P("tp", None),
        P(),
        P("sp", None),
        P("sp", None),
        P("sp", None, "tp"),
        P("sp", None, "tp"),
        P("sp", "tp", None),
    )
    return jax.shard_map(
        functools.partial(layer, mesh.shape["sp"], mesh.shape["tp"]),
        mesh=mesh,
        in_specs=in_specs,
        out_specs=P(("sp", "tp"), None),
        check_vma=False,
    )
```

time: 370 us -> 133 us (0.36)
  blocking collectives: 196 us -> 0 us
  Pallas kernels: 0 us -> 122 us
  waiting for transfers between devices: 103 us -> 0 us
  matrix products: 22.8 us -> 0 us
  other arithmetic: 20.8 us -> 0 us
  between operations: 13.5 us -> 0.01 us
    all_to_all x4 -> x0, blocking collectives: 172 us -> none  [the longest x2 97.7 us: sent_and_summed(): lax.all_to_all(tiles, axis, split_axis=0, concat_axis=0, tiled=True)]
    pallas_call x0 -> x1, Pallas kernels: none -> 122 us  [layer(): pl.pallas_call(functools.partial(layer_kernel, (n_sp, n_tp, rows, width,...]
    all_gather x4 -> x0, waiting for transfers between devices: 102 us -> none  [the longest x2 52.6 us: carried_in(): lax.all_gather(part.astype(kind), axis)]
    all_gather x3 -> x0, blocking collectives: 24.2 us -> none  [the longest x2 22 us: carried_in(): lax.all_gather(part.astype(kind), axis)]
    dot_general x12 -> x0, matrix products: 22.8 us -> none  [the longest x1 4.78 us: body(): jnp.dot(hidden, expert_down[0], preferred_element_type=jnp.float32)]
    unnamed x35 -> x9, local copies, waits for them, and re-layouts: 2.96 us -> 10.9 us
    reduce_sum x5 -> x0, other arithmetic: 6.55 us -> none  [the longest x1 4.15 us: body(): jnp.sum(full_table * route_weights.reshape(length, TOP, 1), axis=1)]
    convert_element_type x11 -> x0, other arithmetic: 4.82 us -> none  [the longest x3 2.9 us: carried_in(): part.astype(kind)]
  transfers between devices with their start and end apart: 4 -> 0, of which waited for: 4 -> 0; matrix products, arithmetic and copies ran while one was open for 4% -> 0% of each run, Pallas kernels for 0% -> 0%
where the time goes in v1:
time: 133 us
  Pallas kernels  122 us (92%)
  local copies, waits for them, and re-layouts  10.9 us (8%)
    pallas_call x1, Pallas kernels, layer(): pl.pallas_call(functools.partial(layer_kernel, (n_sp, n_tp, rows, width,...  122 us
    unnamed x9, local copies, waits for them, and re-layouts  10.9 us

profile of v1, /device:TPU:1, one launch (start us, length us, event | category | flops | bytes accessed | tf_op | source)
XLA Modules:
  0.0 133.1 jit_solution(14794293976087479908)
XLA Ops:
  0.0 0.0 copy-start
  0.0 1.5 %copy.17.decay_low = bf16[256,16]{1,0:T(8,128)(2,1)} copy(bf16[256,16]{0,1:T(8,128)(2,1)} %param.20) | data formatting | bytes 16384 | tf_op args[4]
  1.5 1.5 %copy.18.decay_shift = f32[256,1]{1,0:T(8,128)} copy(f32[256,1]{0,1:T(1,128)} %param.23) | data formatting | bytes 2048 | tf_op args[7]
  3.0 1.5 %copy.19.routes = s32[256,2]{1,0:T(8,128)} copy(s32[256,2]{0,1:T(2,128)} %param.27) | data formatting | bytes 4096 | tf_op args[11]
  4.5 1.5 %copy.20.route_weights = f32[256,2]{1,0:T(8,128)} copy(f32[256,2]{0,1:T(2,128)} %param.28) | data formatting | bytes 4096 | tf_op args[12]
  5.9 2.2 %copy.21.gate_any = bf16[1,2048,176]{2,1,0:T(8,128)(2,1)} copy(bf16[1,2048,176]{1,2,0:T(8,128)(2,1)} %param.29) | data formatting | bytes 1441792 | tf_op args[13]
  8.1 0.0 copy-done
  8.2 1.3 copy.22.up_any
  9.5 122.2 %layer.1 = bf16[16,2048]{1,0:T(8,128)(2,1)} custom-call(bf16[16,2048]{1,0:T(8,128)(2,1)} %stream.1, bf16[256,256]{1,0:T(8,128)(2,1)} %queries.1, bf16[256,256]{1,0:T(8,128)(2,1)} %key_rows.1, bf16[256,512]{1,0:T(8,128)(2,1)} %values.1, bf16[256,16]{1,0:T(8,128)(2,1)} %copy.17.decay_low, bf16[16,256]{1,0:T(8,128)(2,1)} %decay_matrix.1, f32[1,256]{1,0:T(1,128)} %bitcast.5, ...), custom_call_target="tpu_custom_call" | custom-call | tf_op jit(solution)/shard_map/layer/pallas_call | solution.py:679
  131.6 1.5 %copy.24 = bf16[16,2048]{1,0:T(8,128)(2,1)} copy(bf16[16,2048]{1,0:T(8,128)(2,1)} %layer.1) | data formatting | bytes 131072
Async XLA Ops:
  0.0 8.1 %copy-start = (bf16[1,2048,176]{1,2,0:T(8,128)(2,1)S(1)}, bf16[1,2048,176]{1,2,0:T(8,128)(2,1)}, u32[]{:S(2)}) copy-start(bf16[1,2048,176]{1,2,0:T(8,128)(2,1)} %param.30) | copy-start | bytes 2162692

commit v2 on v1

--- a/solution.py
+++ b/solution.py
@@ -148,6 +148,7 @@
     other = 1 - core
     mate = (sp, tp + 1 - 2 * core)
 
+    pending = []
     loads = []
     for i, (src, dst) in enumerate(
         (
@@ -183,10 +184,18 @@
     lax.fori_loop(1, n_sp, greet_sp, 0)
     lax.fori_loop(1, n_tp, greet_tp, 0)
 
-    before_gate = dot(decay_low[...], decay_matrix[...]) + decay_bias[...]
+    line = iota((BLK, length), 0)
+    lines = jnp.where(line == 0, decay_shift[...], 0.0)
+    for i, row in enumerate((routes[0:1, :].astype(F32), routes[1:2, :].astype(F32))):
+        lines = jnp.where(line == 1 + i, row, lines)
+    for i in range(2):
+        lines = jnp.where(line == 3 + i, route_weights[i : i + 1, :], lines)
+    table = lines.T
+    low_rows = decay_low[...].astype(F32).T.astype(BF)
+    before_gate = dot(low_rows, decay_matrix[...]) + decay_bias[...]
     logs = (
         jnp.minimum(before_gate, 0.0) - jnp.log1p(jnp.exp(-jnp.abs(before_gate)))
-    ) / TEMPER + decay_shift[...]
+    ) / TEMPER + table[:, 0:1]
     lower = iota((BLK, BLK), 0) >= iota((BLK, BLK), 1)
     lower_ones = jnp.where(lower, 1.0, 0.0).astype(BF)
     inside = []
@@ -228,6 +237,12 @@
         return carry
 
     lax.fori_loop(1, n_sp, send_state, 0)
+    most = pl.ds(0, n_sp - 1)
+    pending.append(
+        remote(
+            state_send.at[most], state_recv.at[most], state_ss, state_rs.at[0], mate
+        ).wait_send
+    )
     state_recv[sp] = state_send[sp]
 
     for n in range(2):
@@ -248,9 +263,9 @@
         total_s[block, :] = total
         query_s[block, :] = query
 
-    expert = iota((length, n_sp), 1)
-    first = jnp.where(routes[:, 0:1] == expert, 1.0, 0.0)
-    second = jnp.where(routes[:, 1:2] == expert, 1.0, 0.0)
+    expert = iota((length, n_sp), 1).astype(F32)
+    first = jnp.where(table[:, 1:2] == expert, 1.0, 0.0)
+    second = jnp.where(table[:, 2:3] == expert, 1.0, 0.0)
     named = first + second
     earlier = jnp.where(iota((length, length), 0) > iota((length, length), 1), 1.0, 0.0)
     rank = dot(earlier.astype(BF), named.astype(BF))
@@ -266,12 +281,10 @@
     spread = jnp.where((at >= start) & (at < start + slots), 1.0, 0.0).astype(BF)
     slot = ((iota((length, count), 1) & (slots - 1)) + 1).astype(F32)
     chosen = dot(place, spread) == slot
-    high, low = split2(first * route_weights[:, 0:1] + second * route_weights[:, 1:2])
+    high, low = split2(first * table[:, 3:4] + second * table[:, 4:5])
     weight_high[...] = jnp.where(chosen, dot(high, spread), 0.0).astype(BF)
     weight_low[...] = jnp.where(chosen, dot(low, spread), 0.0).astype(BF)
 
-    for n in range(PARTS):
-        row_recv[n, y] = jnp.zeros(row_recv.shape[2:], BF)
     down_s[piece:, :] = jnp.zeros((down_s.shape[0] - piece, width), BF)
     hidden_s[...] = jnp.zeros(hidden_s.shape, BF)
 
@@ -296,10 +309,11 @@
         return state * decay + came[:, :hv]
 
     lax.fori_loop(0, n_sp, carry_state, jnp.zeros((hk // n_sp, hv), F32))
-    most = pl.ds(0, n_sp - 1)
-    remote(
+    prior_all = remote(
         prior_send.at[most], prior_recv.at[most], prior_ss, prior_rs, mate
-    ).wait_recv()
+    )
+    prior_all.wait_recv()
+    pending.append(prior_all.wait_send)
     carried = prior_recv[...].astype(F32).reshape(hk, hv).astype(BF)
     high, low = split2(query_s[...])
     total = total_s[...] + (dot(high, carried) + dot(low, carried))
@@ -315,29 +329,34 @@
             lax.rem(i, 2) == 0, half_ring + lax.div(i, 2), half_ring - lax.div(i + 1, 2)
         )
 
+    right = (sp, 2 * lax.rem(y + 1, n_y) + core)
+    left = (sp, 2 * lax.rem(y + n_y - 1, n_y) + core)
+    toward = (right, left)
+
     def pair_copy(n):
         return remote(
             pair_send.at[n], pair_recv.at[n], pair_ss.at[n], pair_rs.at[n], mate
         )
 
+    def hop_copy(d, k, n):
+        return remote(
+            row_send.at[d, k, n],
+            row_recv.at[d, k, n],
+            row_ss.at[d, k, n],
+            row_rs.at[d, k, n],
+            toward[d],
+        )
+
     def add_pair(n):
         pair_copy(n).wait_recv()
-        total = own_s[n] + pair_recv[n].astype(F32)
-        own_s[n] = total
-        row_send[n] = total.astype(BF)
-
-        def send_row(i, carry):
-            yy = lax.rem(y + order(i), n_y)
-            remote(
-                row_send.at[n, yy],
-                row_recv.at[n, y],
-                row_ss.at[n],
-                row_rs.at[n],
-                (sp, 2 * yy + core),
-            ).start()
-            return carry
-
-        lax.fori_loop(0, n_y - 1, send_row, 0)
+        own_s[n] = own_s[n] + pair_recv[n].astype(F32)
+        far = own_s[n, lax.rem(y + half_ring, n_y)].astype(BF)
+        for d in range(2):
+
+            @pl.when(lax.div(n, PARTS // 2) == d)
+            def _():
+                row_send[d, 0, n] = far
+                hop_copy(d, 0, n).start()
 
     loads[0].wait()
 
@@ -358,14 +377,40 @@
 
     lax.fori_loop(0, PARTS, project, 0)
     add_pair(PARTS - 1)
-
-    rest = pl.ds(0, n_y - 1)
+    pending += [pair_copy(n).wait_send for n in range(PARTS)]
+
+    def pass_rows(k, carry):
+        for n in range(PARTS):
+            for d in range(2):
+                hold = lax.rem(y + n_y + (1 - 2 * d) * (half_ring - k), n_y)
+                comes = n // (PARTS // 2) == d
+
+                @pl.when(jnp.logical_or(k > 1, comes))
+                def _():
+                    hop_copy(d, k - 1, n).wait_recv()
+                    total = own_s[n, hold] + row_recv[d, k - 1, n].astype(F32)
+                    row_send[d, k, n] = total.astype(BF)
+
+                if not comes:
+
+                    @pl.when(k == 1)
+                    def _():
+                        row_send[d, k, n] = own_s[n, hold].astype(BF)
+
+                hop_copy(d, k, n).start()
+        return carry
+
+    lax.fori_loop(1, half_ring, pass_rows, 0)
     for n in range(PARTS):
         lanes = slice(n * part_width, (n + 1) * part_width)
-        remote(
-            row_send.at[n, rest], row_recv.at[n, rest], row_ss.at[n], row_rs.at[n], mate
-        ).wait_recv()
-        total = own_s[n, y] + jnp.sum(row_recv[n].astype(F32), axis=0)
+        total = own_s[n, y]
+        for d in range(2):
+            if half_ring > 1 or n // (PARTS // 2) == d:
+                hop_copy(d, half_ring - 1, n).wait_recv()
+                total += row_recv[d, half_ring - 1, n].astype(F32)
+            for k in range(half_ring):
+                if k > 0 or n // (PARTS // 2) == d:
+                    pending.append(hop_copy(d, k, n).wait_send)
         mid_s[:, lanes] = stream[:, lanes].astype(F32) + total
     middle = mid_s[...]
     normed = (
@@ -388,6 +433,7 @@
         return remote(send.at[others], recv.at[others], send_sem, recv_sem, mate)
 
     norm_all = to_tp(norm_send, norm_recv, norm_ss, norm_rs)
+    pending.append(norm_all.wait_send)
     norm_all.wait_recv()
     group = norm_recv[...].reshape(length, columns)
     slot_send[...] = dot(select_s[...], group).astype(BF).reshape(n_sp, slots, columns)
@@ -404,6 +450,11 @@
         return carry
 
     lax.fori_loop(1, n_sp, send_slots, 0)
+    pending.append(
+        remote(
+            slot_send.at[most], rows_s.at[0, 0, most], slot_ss, slot_rs.at[0], mate
+        ).wait_send
+    )
     rows_s[y, core, sp] = slot_send[sp]
 
     n_half = n_sp // 2
@@ -460,9 +511,16 @@
                 else:
                     pl.when(step < half_ring)(one)
 
-    loads[1].wait()
-    loads[2].wait()
-    loads[3].wait()
+    for step in range(1, half_ring + 1):
+        for d in range(2):
+            for p in range(2):
+                if step < half_ring or d == p:
+                    pending.append(ring_copy(d, step, p).wait_send)
+    for i in range(n_y):
+        for p in range(2):
+            pending.append(mate_copy(i, core, p).wait_send)
+    for load in loads[1:]:
+        load.wait()
     gate_acc[...] = jnp.zeros(gate_acc.shape, F32)
     up_acc[...] = jnp.zeros(up_acc.shape, F32)
 
@@ -482,8 +540,8 @@
             axis=1,
         )
         depth = pl.ds(pl.multiple_of(yy * 2 * columns, 2 * columns), 2 * columns)
-        gate_acc[...] += dot(x, gate_s[depth, :])
-        up_acc[...] += dot(x, up_s[depth, :])
+        gate_acc[...] += dot_nt(x, gate_s[:, depth])
+        up_acc[...] += dot_nt(x, up_s[:, depth])
         return carry
 
     lax.fori_loop(0, n_y, widen, 0)
@@ -496,27 +554,54 @@
             half_send.at[i], half_recv.at[i], half_ss.at[i], half_rs.at[i], mate
         )
 
+    def sum_copy(d, k, p):
+        to = lax.rem(y + n_y + 1 - 2 * d, n_y)
+        return remote(
+            sum_send.at[d, k, p],
+            sum_recv.at[d, k, p],
+            sum_ss.at[d, k, p],
+            sum_rs.at[d, k, p],
+            (sp, 2 * to + core),
+        )
+
     def add_half(i):
-        yy = lax.rem(y + order(i), n_y)
         half_copy(i).wait_recv()
-        total = half_own[i] + half_recv[i].astype(F32)
-        half_own[i] = total
-
-        @pl.when(i < n_y - 1)
+
+        @pl.when(i == 0)
         def _():
-            sum_send[i] = total.astype(BF)
-            remote(
-                sum_send.at[i], sum_recv.at[y], sum_ss, sum_rs, (sp, 2 * yy + core)
-            ).start()
+            for p in range(2):
+                total = half_own[i, p] + half_recv[i, p].astype(F32)
+                sum_send[p, 0, p] = total.astype(BF)
+                sum_copy(p, 0, p).start()
+
+        @pl.when(i > 0)
+        def _():
+            d = 1 - lax.rem(i, 2)
+            k = lax.div(i + 1, 2)
+            for p in range(2):
+                total = half_own[i, p] + half_recv[i, p].astype(F32)
+
+                @pl.when(jnp.logical_or(k > 1, d == p))
+                def _():
+                    sum_copy(d, k - 1, p).wait_recv()
+                    more = total + sum_recv[d, k - 1, p].astype(F32)
+                    sum_send[d, k, p] = more.astype(BF)
+
+                @pl.when(jnp.logical_and(k == 1, d != p))
+                def _():
+                    sum_send[d, k, p] = total.astype(BF)
+
+                sum_copy(d, k, p).start()
 
     def lower_rows(i, carry):
         yy = lax.rem(y + order(i), n_y)
         lanes = pl.ds(pl.multiple_of(yy * 2 * columns, 2 * columns), 2 * columns)
         product = dot(hidden_s[...], down_s[:, lanes])
         left, right = product[:, :columns], product[:, columns:]
-        half_send[i] = jnp.where(core == 0, right, left).astype(BF)
+        shape = half_send.shape[1:]
+        half_send[i] = jnp.where(core == 0, right, left).astype(BF).reshape(shape)
         half_copy(i).start()
-        half_own[i] = jnp.where(core == 0, left, right).astype(BF).astype(F32)
+        half_own[i] = jnp.where(core == 0, left, right).reshape(shape)
 
         @pl.when(i > 0)
         def _():
@@ -525,11 +610,24 @@
         return carry
 
     lax.fori_loop(0, n_y, lower_rows, 0)
-    sum_recv[y] = jnp.zeros(sum_recv.shape[1:], BF)
-    add_half(n_y - 1)
-    remote(sum_send, sum_recv.at[rest], sum_ss, sum_rs, mate).wait_recv()
-    total = half_own[n_y - 1] + jnp.sum(sum_recv[...].astype(F32), axis=0)
-    back_send[...] = total.astype(BF).reshape(n_sp, slots, columns)
+    last = n_y - 1
+    half_copy(last).wait_recv()
+    for p in range(2):
+        total = half_own[last, p] + half_recv[last, p].astype(F32)
+        for d in range(2):
+            if half_ring > 1 or d == p:
+                sum_copy(d, half_ring - 1, p).wait_recv()
+                total += sum_recv[d, half_ring - 1, p].astype(F32)
+        back_send[p * n_half : (p + 1) * n_half] = total.astype(BF).reshape(
+            n_half, slots, columns
+        )
+    for i in range(n_y):
+        pending.append(half_copy(i).wait_send)
+    for d in range(2):
+        for k in range(half_ring):
+            for p in range(2):
+                if k > 0 or d == p:
+                    pending.append(sum_copy(d, k, p).wait_send)
 
     def send_back(i, carry):
         peer = lax.rem(sp + i, n_sp)
@@ -538,41 +636,21 @@
 
     lax.fori_loop(1, n_sp, send_back, 0)
     back_recv[sp] = back_send[sp]
-    remote(back_send.at[most], back_recv.at[most], back_ss, back_rs, mate).wait_recv()
+    back_all = remote(back_send.at[most], back_recv.at[most], back_ss, back_rs, mate)
+    pending.append(back_all.wait_send)
+    back_all.wait_recv()
     returned = back_recv[...].reshape(count, columns)
     routed = dot(weight_high[...], returned) + dot(weight_low[...], returned)
     last_send[...] = routed.astype(BF).reshape(n_tp, rows, columns)
     last_all = to_tp(last_send, last_recv, last_ss, last_rs)
+    pending.append(last_all.wait_send)
     last_all.wait_recv()
     for j in range(n_tp):
         lanes = slice(j * columns, (j + 1) * columns)
         out[:, lanes] = (mid_s[:, lanes] + last_recv[j].astype(F32)).astype(BF)
 
-    remote(
-        state_send.at[most], state_recv.at[most], state_ss, state_rs.at[0], mate
-    ).wait_send()
-    remote(prior_send.at[most], prior_recv.at[most], prior_ss, prior_rs, mate).wait_send()
-    for n in range(PARTS):
-        pair_copy(n).wait_send()
-        remote(
-            row_send.at[n, rest], row_recv.at[n, rest], row_ss.at[n], row_rs.at[n], mate
-        ).wait_send()
-    norm_all.wait_send()
-    remote(
-        slot_send.at[most], rows_s.at[0, 0, most], slot_ss, slot_rs.at[0], mate
-    ).wait_send()
-    for step in range(1, half_ring + 1):
-        for d in range(2):
-            for p in range(2):
-                if step < half_ring or d == p:
-                    ring_copy(d, step, p).wait_send()
-    for yy in range(n_y):
-        for p in range(2):
-            mate_copy(yy, core, p).wait_send()
-        half_copy(yy).wait_send()
-    remote(sum_send, sum_recv.at[rest], sum_ss, sum_rs, mate).wait_send()
-    remote(back_send.at[most], back_recv.at[most], back_ss, back_rs, mate).wait_send()
-    last_all.wait_send()
+    for finish in pending:
+        finish()
 
 
 def layer(
@@ -614,8 +692,8 @@
     dma = pltpu.SemaphoreType.DMA
     scratch = [
         pltpu.VMEM((hv, width), BF),
-        pltpu.VMEM((width, piece), BF),
-        pltpu.VMEM((width, piece), BF),
+        pltpu.VMEM((piece, width), BF),
+        pltpu.VMEM((piece, width), BF),
         pltpu.VMEM((padded, width), BF),
         pltpu.VMEM((length, hk), F32),
         pltpu.VMEM((length, hv), F32),
@@ -631,8 +709,8 @@
         pltpu.VMEM((PARTS, n_y, rows, part), BF),
         pltpu.VMEM((PARTS, n_y, rows, part), BF),
         pltpu.VMEM((PARTS, n_y, rows, part), F32),
-        pltpu.VMEM((PARTS, n_y, rows, part), BF),
-        pltpu.VMEM((PARTS, n_y, rows, part), BF),
+        pltpu.VMEM((2, half_ring, PARTS, rows, part), BF),
+        pltpu.VMEM((2, half_ring, PARTS, rows, part), BF),
         pltpu.VMEM((rows, width), F32),
         pltpu.VMEM((n_tp, rows, columns), BF),
         pltpu.VMEM((n_tp, rows, columns), BF),
@@ -641,11 +719,11 @@
         pltpu.VMEM((count, piece), F32),
         pltpu.VMEM((count, piece), F32),
         pltpu.VMEM((count, padded), BF),
-        pltpu.VMEM((n_y, count, columns), BF),
-        pltpu.VMEM((n_y, count, columns), BF),
-        pltpu.VMEM((n_y, count, columns), F32),
-        pltpu.VMEM((n_y - 1, count, columns), BF),
-        pltpu.VMEM((n_y, count, columns), BF),
+        pltpu.VMEM((n_y, 2, count // 2, columns), BF),
+        pltpu.VMEM((n_y, 2, count // 2, columns), BF),
+        pltpu.VMEM((n_y, 2, count // 2, columns), F32),
+        pltpu.VMEM((2, half_ring, 2, count // 2, columns), BF),
+        pltpu.VMEM((2, half_ring, 2, count // 2, columns), BF),
         pltpu.VMEM((n_sp, slots, columns), BF),
         pltpu.VMEM((n_sp, slots, columns), BF),
         pltpu.VMEM((n_tp, rows, columns), BF),
@@ -657,8 +735,8 @@
         dma,
         dma((PARTS,)),
         dma((PARTS,)),
-        dma((PARTS,)),
-        dma((PARTS,)),
+        dma((2, half_ring, PARTS)),
+        dma((2, half_ring, PARTS)),
         dma,
         dma,
         dma,
@@ -669,8 +747,8 @@
         dma((n_y, 2)),
         dma((n_y,)),
         dma((n_y,)),
-        dma,
-        dma,
+        dma((2, half_ring, 2)),
+        dma((2, half_ring, 2)),
         dma,
         dma,
         dma,
@@ -691,17 +769,17 @@
         queries,
         key_rows,
         values,
-        decay_low,
+        decay_low.T,
         decay_matrix,
         decay_bias.reshape(1, -1),
-        decay_shift,
+        decay_shift.T,
         head_gain.reshape(1, -1),
         output_matrix,
         feed_gain.reshape(1, -1),
-        routes,
-        route_weights,
-        expert_gate,
-        specialist_widen,
+        routes.T,
+        route_weights.T,
+        jnp.swapaxes(expert_gate, 1, 2),
+        jnp.swapaxes(specialist_widen, 1, 2),
         expert_down,
     )
 

time: 133 us -> 117 us (0.88)
  local copies, waits for them, and re-layouts: 10.9 us -> 1.47 us
  Pallas kernels: 122 us -> 115 us
    unnamed x9 -> x1, local copies, waits for them, and re-layouts: 10.9 us -> 1.47 us
    pallas_call x1, Pallas kernels: 122 us -> 115 us  [layer(): pl.pallas_call(functools.partial(layer_kernel, (n_sp, n_tp, rows, width,...]
where the time goes in v2:
time: 117 us; the launch traced here: 116 us
  Pallas kernels  115 us (98%)
  local copies, waits for them, and re-layouts  1.47 us (1%)
    pallas_call x1, Pallas kernels, layer(): pl.pallas_call(functools.partial(layer_kernel, (n_sp, n_tp, rows, width,...  115 us

profile of v2, /device:TPU:1, one launch (start us, length us, event | category | flops | bytes accessed | tf_op | source)
XLA Modules:
  0.0 116.4 jit_solution(18269284722141716817)
XLA Ops:
  0.0 114.9 %layer.1 = bf16[16,2048]{1,0:T(8,128)(2,1)} custom-call(bf16[16,2048]{1,0:T(8,128)(2,1)} %stream.1, bf16[256,256]{1,0:T(8,128)(2,1)} %queries.1, bf16[256,256]{1,0:T(8,128)(2,1)} %key_rows.1, bf16[256,512]{1,0:T(8,128)(2,1)} %values.1, bf16[16,256]{1,0:T(8,128)(2,1)} %bitcast.11, bf16[16,256]{1,0:T(8,128)(2,1)} %decay_matrix.1, f32[1,256]{1,0:T(1,128)} %bitcast.16, ...), custom_call_target="tpu_custom_call" | custom-call | tf_op jit(solution)/shard_map/layer/pallas_call | solution.py:757
  114.9 1.5 %copy.18 = bf16[16,2048]{1,0:T(8,128)(2,1)} copy(bf16[16,2048]{1,0:T(8,128)(2,1)} %layer.1) | data formatting | bytes 131072

commit v3 on v2

--- a/solution.py
+++ b/solution.py
@@ -10,7 +10,7 @@
 BLK = 128
 TEMPER = 16.0
 EPSILON = 1e-06
-PARTS = 4
+PIECES = 4
 BF = jnp.bfloat16
 F32 = jnp.float32
 
@@ -84,14 +84,18 @@
     weight_high,
     weight_low,
     mixed_s,
-    pair_send,
-    pair_recv,
-    own_s,
+    first_send,
+    first_recv,
     row_send,
     row_recv,
+    row_own,
+    row_out,
+    row_in,
     mid_s,
-    norm_send,
-    norm_recv,
+    square_send,
+    square_recv,
+    scale_send,
+    scale_recv,
     slot_send,
     rows_s,
     gate_acc,
@@ -100,8 +104,8 @@
     half_send,
     half_recv,
     half_own,
-    sum_send,
-    sum_recv,
+    sum_out,
+    sum_in,
     back_send,
     back_recv,
     last_send,
@@ -111,12 +115,16 @@
     state_rs,
     prior_ss,
     prior_rs,
-    pair_ss,
-    pair_rs,
+    first_ss,
+    first_rs,
     row_ss,
     row_rs,
-    norm_ss,
-    norm_rs,
+    hop_ss,
+    hop_rs,
+    square_ss,
+    square_rs,
+    scale_ss,
+    scale_rs,
     slot_ss,
     slot_rs,
     ring_ss,
@@ -138,7 +146,8 @@
     length = rows * n_tp
     slots = 2 * length // n_sp
     columns = width // n_tp
-    part_width = width // PARTS
+    count = n_sp * slots
+    pieces = min(PIECES, n_sp)
     hk = queries.shape[1]
     hv = values.shape[1]
     sp = lax.axis_index("sp")
@@ -227,6 +236,8 @@
     )
     state_send[:, :, hv : hv + BLK] = packed.reshape(n_sp, hk // n_sp, BLK).astype(BF)
 
+    for j in range(n_tp):
+        first_send[j] = stream[:, j * columns : (j + 1) * columns]
     pl.semaphore_wait(barrier, n_sp - 1 + n_tp - 1)
 
     def send_state(i, carry):
@@ -244,6 +255,33 @@
         ).wait_send
     )
     state_recv[sp] = state_send[sp]
+
+    def to_tp(send, recv, send_sem, recv_sem):
+        def start(i, carry):
+            peer = lax.rem(tp + i, n_tp)
+            remote(send.at[peer], recv.at[tp], send_sem, recv_sem, (sp, peer)).start()
+            return carry
+
+        lax.fori_loop(1, n_tp, start, 0)
+        recv[tp] = send[tp]
+        others = pl.ds(0, n_tp - 1)
+        every = remote(send.at[others], recv.at[others], send_sem, recv_sem, mate)
+        pending.append(every.wait_send)
+        return every
+
+    def to_sp(send, recv, send_sem, recv_sem):
+        def start(i, carry):
+            peer = lax.rem(sp + i, n_sp)
+            remote(send.at[peer], recv.at[sp], send_sem, recv_sem, (peer, tp)).start()
+            return carry
+
+        lax.fori_loop(1, n_sp, start, 0)
+        recv[sp] = send[sp]
+        every = remote(send.at[most], recv.at[most], send_sem, recv_sem, mate)
+        pending.append(every.wait_send)
+        return every
+
+    first_all = to_tp(first_send, first_recv, first_ss, first_rs)
 
     for n in range(2):
         block = slice(n * BLK, (n + 1) * BLK)
@@ -270,7 +308,6 @@
     earlier = jnp.where(iota((length, length), 0) > iota((length, length), 1), 1.0, 0.0)
     rank = dot(earlier.astype(BF), named.astype(BF))
     place = (named * (rank + 1.0)).astype(BF)
-    count = n_sp * slots
     start = iota((count, n_sp), 1) * slots
     at = iota((count, n_sp), 0)
     spread = jnp.where((at >= start) & (at < start + slots), 1.0, 0.0).astype(BF)
@@ -322,120 +359,120 @@
         * lax.rsqrt(jnp.mean(total * total, axis=-1, keepdims=True) + EPSILON)
         * head_gain[...]
     ).astype(BF)
-    mixed_s[...] = mixed.reshape(n_y, 2, rows, hv)
+    mixed_s[...] = mixed
 
     def order(i):
         return jnp.where(
             lax.rem(i, 2) == 0, half_ring + lax.div(i, 2), half_ring - lax.div(i + 1, 2)
         )
 
-    right = (sp, 2 * lax.rem(y + 1, n_y) + core)
-    left = (sp, 2 * lax.rem(y + n_y - 1, n_y) + core)
-    toward = (right, left)
-
-    def pair_copy(n):
-        return remote(
-            pair_send.at[n], pair_recv.at[n], pair_ss.at[n], pair_rs.at[n], mate
-        )
-
-    def hop_copy(d, k, n):
-        return remote(
-            row_send.at[d, k, n],
-            row_recv.at[d, k, n],
-            row_ss.at[d, k, n],
-            row_rs.at[d, k, n],
-            toward[d],
-        )
-
-    def add_pair(n):
-        pair_copy(n).wait_recv()
-        own_s[n] = own_s[n] + pair_recv[n].astype(F32)
-        far = own_s[n, lax.rem(y + half_ring, n_y)].astype(BF)
+    def summed_product(left_ref, right_ref, send, recv, own, out_buf, in_buf, sems):
+        mate_send, mate_recv, hop_send, hop_recv = sems
+        shape = send.shape[1:]
+        first_way = shape[0] // 2
+
+        def share(i):
+            return remote(send.at[i], recv.at[i], mate_send.at[i], mate_recv.at[i], mate)
+
+        def hop(d, k, p):
+            to = lax.rem(y + n_y + 1 - 2 * d, n_y)
+            return remote(
+                out_buf.at[d, k, p],
+                in_buf.at[d, k, p],
+                hop_send.at[d, k, p],
+                hop_recv.at[d, k, p],
+                (sp, 2 * to + core),
+            )
+
+        def add(i):
+            share(i).wait_recv()
+
+            @pl.when(i == 0)
+            def _():
+                for p in range(shape[0]):
+                    d = p // first_way
+                    total = own[i, p] + recv[i, p].astype(F32)
+                    out_buf[d, 0, p] = total.astype(BF)
+                    hop(d, 0, p).start()
+
+            @pl.when(i > 0)
+            def _():
+                d = 1 - lax.rem(i, 2)
+                k = lax.div(i + 1, 2)
+                for p in range(shape[0]):
+                    total = own[i, p] + recv[i, p].astype(F32)
+                    comes = jnp.logical_or(k > 1, d == p // first_way)
+
+                    @pl.when(comes)
+                    def _():
+                        hop(d, k - 1, p).wait_recv()
+                        more = total + in_buf[d, k - 1, p].astype(F32)
+                        out_buf[d, k, p] = more.astype(BF)
+
+                    @pl.when(jnp.logical_not(comes))
+                    def _():
+                        out_buf[d, k, p] = total.astype(BF)
+
+                    hop(d, k, p).start()
+
+        def multiply(i, carry):
+            yy = lax.rem(y + order(i), n_y)
+            lanes = pl.ds(pl.multiple_of(yy * 2 * columns, 2 * columns), 2 * columns)
+            product = dot(left_ref[...], right_ref[:, lanes])
+            low, high = product[:, :columns], product[:, columns:]
+            send[i] = jnp.where(core == 0, high, low).astype(BF).reshape(shape)
+            share(i).start()
+            own[i] = jnp.where(core == 0, low, high).reshape(shape)
+
+            @pl.when(i > 0)
+            def _():
+                add(i - 1)
+
+            return carry
+
+        lax.fori_loop(0, n_y, multiply, 0)
+        last = n_y - 1
+        share(last).wait_recv()
+        totals = []
+        for p in range(shape[0]):
+            total = own[last, p] + recv[last, p].astype(F32)
+            for d in range(2):
+                if half_ring > 1 or d == p // first_way:
+                    hop(d, half_ring - 1, p).wait_recv()
+                    total += in_buf[d, half_ring - 1, p].astype(F32)
+            totals.append(total)
+        for i in range(n_y):
+            pending.append(share(i).wait_send)
         for d in range(2):
-
-            @pl.when(lax.div(n, PARTS // 2) == d)
-            def _():
-                row_send[d, 0, n] = far
-                hop_copy(d, 0, n).start()
+            for k in range(half_ring):
+                for p in range(shape[0]):
+                    if k > 0 or d == p // first_way:
+                        pending.append(hop(d, k, p).wait_send)
+        return jnp.concatenate(totals, axis=0)
 
     loads[0].wait()
-
-    def project(n, carry):
-        lanes = pl.ds(pl.multiple_of(n * part_width, part_width), part_width)
-        theirs = mixed_s[:, other].reshape(n_y * rows, hv)
-        pair_send[n] = dot(theirs, w_s[:, lanes]).astype(BF).reshape(n_y, rows, part_width)
-        pair_copy(n).start()
-        mine = mixed_s[:, core].reshape(n_y * rows, hv)
-        product = dot(mine, w_s[:, lanes]).astype(BF).astype(F32)
-        own_s[n] = product.reshape(n_y, rows, part_width)
-
-        @pl.when(n > 0)
-        def _():
-            add_pair(n - 1)
-
-        return carry
-
-    lax.fori_loop(0, PARTS, project, 0)
-    add_pair(PARTS - 1)
-    pending += [pair_copy(n).wait_send for n in range(PARTS)]
-
-    def pass_rows(k, carry):
-        for n in range(PARTS):
-            for d in range(2):
-                hold = lax.rem(y + n_y + (1 - 2 * d) * (half_ring - k), n_y)
-                comes = n // (PARTS // 2) == d
-
-                @pl.when(jnp.logical_or(k > 1, comes))
-                def _():
-                    hop_copy(d, k - 1, n).wait_recv()
-                    total = own_s[n, hold] + row_recv[d, k - 1, n].astype(F32)
-                    row_send[d, k, n] = total.astype(BF)
-
-                if not comes:
-
-                    @pl.when(k == 1)
-                    def _():
-                        row_send[d, k, n] = own_s[n, hold].astype(BF)
-
-                hop_copy(d, k, n).start()
-        return carry
-
-    lax.fori_loop(1, half_ring, pass_rows, 0)
-    for n in range(PARTS):
-        lanes = slice(n * part_width, (n + 1) * part_width)
-        total = own_s[n, y]
-        for d in range(2):
-            if half_ring > 1 or n // (PARTS // 2) == d:
-                hop_copy(d, half_ring - 1, n).wait_recv()
-                total += row_recv[d, half_ring - 1, n].astype(F32)
-            for k in range(half_ring):
-                if k > 0 or n // (PARTS // 2) == d:
-                    pending.append(hop_copy(d, k, n).wait_send)
-        mid_s[:, lanes] = stream[:, lanes].astype(F32) + total
-    middle = mid_s[...]
-    normed = (
-        middle
-        * lax.rsqrt(jnp.mean(middle * middle, axis=-1, keepdims=True) + EPSILON)
-        * feed_gain[...]
-    ).astype(BF)
+    attended = summed_product(
+        mixed_s,
+        w_s,
+        row_send,
+        row_recv,
+        row_own,
+        row_out,
+        row_in,
+        (row_ss, row_rs, hop_ss, hop_rs),
+    )
+    first_all.wait_recv()
+    middle = attended + first_recv[...].astype(F32).reshape(length, columns)
+    mid_s[...] = middle
+    high, low = split2(middle * middle)
+    ones = jnp.ones((8, columns), BF)
+    squares = (dot_nt(ones, high) + dot_nt(ones, low))[0:1, :]
     for j in range(n_tp):
-        norm_send[j] = normed[:, j * columns : (j + 1) * columns]
-
-    def to_tp(send, recv, send_sem, recv_sem):
-        def start(i, carry):
-            peer = lax.rem(tp + i, n_tp)
-            remote(send.at[peer], recv.at[tp], send_sem, recv_sem, (sp, peer)).start()
-            return carry
-
-        lax.fori_loop(1, n_tp, start, 0)
-        recv[tp] = send[tp]
-        others = pl.ds(0, n_tp - 1)
-        return remote(send.at[others], recv.at[others], send_sem, recv_sem, mate)
-
-    norm_all = to_tp(norm_send, norm_recv, norm_ss, norm_rs)
-    pending.append(norm_all.wait_send)
-    norm_all.wait_recv()
-    group = norm_recv[...].reshape(length, columns)
+        square_send[j] = squares
+    square_all = to_tp(square_send, square_recv, square_ss, square_rs)
+
+    own_lanes = pl.ds(pl.multiple_of(tp * columns, columns), columns)
+    group = (middle * feed_gain[:, own_lanes]).astype(BF)
     slot_send[...] = dot(select_s[...], group).astype(BF).reshape(n_sp, slots, columns)
 
     def send_slots(i, carry):
@@ -457,21 +494,24 @@
     )
     rows_s[y, core, sp] = slot_send[sp]
 
-    n_half = n_sp // 2
+    n_part = n_sp // pieces
 
     def ring_copy(d, step, p):
         yy = lax.rem(y + n_y + (1 - 2 * d) * (1 - step), n_y)
         to = lax.rem(y + n_y + 1 - 2 * d, n_y)
-        part = rows_s.at[yy, core, pl.ds(p * n_half, n_half)]
+        part = rows_s.at[yy, core, pl.ds(p * n_part, n_part)]
         return remote(
             part, part, ring_ss.at[d, step, p], ring_rs.at[d, step, p], (sp, 2 * to + core)
         )
 
     def mate_copy(yy, c, p):
-        part = rows_s.at[yy, c, pl.ds(p * n_half, n_half)]
+        part = rows_s.at[yy, c, pl.ds(p * n_part, n_part)]
         return remote(part, part, mate_ss.at[yy, p], mate_rs.at[yy, p], mate)
 
-    for p in range(2):
+    def ahead(p):
+        return p // (pieces // 2)
+
+    for p in range(pieces):
 
         def wait_slots(b, carry):
             @pl.when(b != sp)
@@ -482,20 +522,20 @@
 
             return carry
 
-        lax.fori_loop(p * n_half, (p + 1) * n_half, wait_slots, 0)
+        lax.fori_loop(p * n_part, (p + 1) * n_part, wait_slots, 0)
         for d in range(2):
-            if half_ring > 1 or d == p:
+            if half_ring > 1 or d == ahead(p):
                 ring_copy(d, 1, p).start()
         mate_copy(y, core, p).start()
 
     def pass_on(step):
-        for p in range(2):
+        for p in range(pieces):
             for d in range(2):
 
                 def one():
                     yy = lax.rem(y + n_y - (1 - 2 * d) * step, n_y)
                     ring_copy(d, step, p).wait_recv()
-                    if d == p:
+                    if d == ahead(p):
                         more = step < half_ring
                     else:
                         more = step + 1 < half_ring
@@ -506,19 +546,27 @@
 
                     mate_copy(yy, core, p).start()
 
-                if d == p:
+                if d == ahead(p):
                     one()
                 else:
                     pl.when(step < half_ring)(one)
 
     for step in range(1, half_ring + 1):
         for d in range(2):
-            for p in range(2):
-                if step < half_ring or d == p:
+            for p in range(pieces):
+                if step < half_ring or d == ahead(p):
                     pending.append(ring_copy(d, step, p).wait_send)
     for i in range(n_y):
-        for p in range(2):
+        for p in range(pieces):
             pending.append(mate_copy(i, core, p).wait_send)
+    square_all.wait_recv()
+    scale = lax.rsqrt(jnp.sum(square_recv[...], axis=0) / width + EPSILON)
+    high, low = split2(jnp.broadcast_to(scale, (BLK, length)).T)
+    packed = jnp.where(
+        iota((length, BLK), 1) < BLK // 2, high.astype(F32), low.astype(F32)
+    ).astype(BF)
+    scale_send[...] = dot(select_s[...], packed).astype(BF).reshape(n_sp, slots, BLK)
+    scale_all = to_sp(scale_send, scale_recv, scale_ss, scale_rs)
     for load in loads[1:]:
         load.wait()
     gate_acc[...] = jnp.zeros(gate_acc.shape, F32)
@@ -533,7 +581,7 @@
 
         offset = jnp.where(lax.rem(m, 2) == 1, -lax.div(m + 1, 2), lax.div(m, 2))
         yy = lax.rem(y + n_y + offset, n_y)
-        for p in range(2):
+        for p in range(pieces):
             mate_copy(yy, other, p).wait_recv()
         x = jnp.concatenate(
             [rows_s[yy, 0].reshape(count, columns), rows_s[yy, 1].reshape(count, columns)],
@@ -545,109 +593,32 @@
         return carry
 
     lax.fori_loop(0, n_y, widen, 0)
-    gated = gate_acc[...]
-    hidden = gated / (1.0 + jnp.exp(-gated)) * up_acc[...]
+    scale_all.wait_recv()
+    packed = scale_recv[...].reshape(count, BLK).astype(F32)
+    scale = packed[:, 0:1] + packed[:, BLK // 2 : BLK // 2 + 1]
+    gated = gate_acc[...] * scale
+    hidden = gated / (1.0 + jnp.exp(-gated)) * (up_acc[...] * scale)
     hidden_s[:, 0:piece] = hidden.astype(BF)
 
-    def half_copy(i):
-        return remote(
-            half_send.at[i], half_recv.at[i], half_ss.at[i], half_rs.at[i], mate
-        )
-
-    def sum_copy(d, k, p):
-        to = lax.rem(y + n_y + 1 - 2 * d, n_y)
-        return remote(
-            sum_send.at[d, k, p],
-            sum_recv.at[d, k, p],
-            sum_ss.at[d, k, p],
-            sum_rs.at[d, k, p],
-            (sp, 2 * to + core),
-        )
-
-    def add_half(i):
-        half_copy(i).wait_recv()
-
-        @pl.when(i == 0)
-        def _():
-            for p in range(2):
-                total = half_own[i, p] + half_recv[i, p].astype(F32)
-                sum_send[p, 0, p] = total.astype(BF)
-                sum_copy(p, 0, p).start()
-
-        @pl.when(i > 0)
-        def _():
-            d = 1 - lax.rem(i, 2)
-            k = lax.div(i + 1, 2)
-            for p in range(2):
-                total = half_own[i, p] + half_recv[i, p].astype(F32)
-
-                @pl.when(jnp.logical_or(k > 1, d == p))
-                def _():
-                    sum_copy(d, k - 1, p).wait_recv()
-                    more = total + sum_recv[d, k - 1, p].astype(F32)
-                    sum_send[d, k, p] = more.astype(BF)
-
-                @pl.when(jnp.logical_and(k == 1, d != p))
-                def _():
-                    sum_send[d, k, p] = total.astype(BF)
-
-                sum_copy(d, k, p).start()
-
-    def lower_rows(i, carry):
-        yy = lax.rem(y + order(i), n_y)
-        lanes = pl.ds(pl.multiple_of(yy * 2 * columns, 2 * columns), 2 * columns)
-        product = dot(hidden_s[...], down_s[:, lanes])
-        left, right = product[:, :columns], product[:, columns:]
-        shape = half_send.shape[1:]
-        half_send[i] = jnp.where(core == 0, right, left).astype(BF).reshape(shape)
-        half_copy(i).start()
-        half_own[i] = jnp.where(core == 0, left, right).reshape(shape)
-
-        @pl.when(i > 0)
-        def _():
-            add_half(i - 1)
-
-        return carry
-
-    lax.fori_loop(0, n_y, lower_rows, 0)
-    last = n_y - 1
-    half_copy(last).wait_recv()
-    for p in range(2):
-        total = half_own[last, p] + half_recv[last, p].astype(F32)
-        for d in range(2):
-            if half_ring > 1 or d == p:
-                sum_copy(d, half_ring - 1, p).wait_recv()
-                total += sum_recv[d, half_ring - 1, p].astype(F32)
-        back_send[p * n_half : (p + 1) * n_half] = total.astype(BF).reshape(
-            n_half, slots, columns
-        )
-    for i in range(n_y):
-        pending.append(half_copy(i).wait_send)
-    for d in range(2):
-        for k in range(half_ring):
-            for p in range(2):
-                if k > 0 or d == p:
-                    pending.append(sum_copy(d, k, p).wait_send)
-
-    def send_back(i, carry):
-        peer = lax.rem(sp + i, n_sp)
-        remote(back_send.at[peer], back_recv.at[sp], back_ss, back_rs, (peer, tp)).start()
-        return carry
-
-    lax.fori_loop(1, n_sp, send_back, 0)
-    back_recv[sp] = back_send[sp]
-    back_all = remote(back_send.at[most], back_recv.at[most], back_ss, back_rs, mate)
-    pending.append(back_all.wait_send)
-    back_all.wait_recv()
+    expert_rows = summed_product(
+        hidden_s,
+        down_s,
+        half_send,
+        half_recv,
+        half_own,
+        sum_out,
+        sum_in,
+        (half_ss, half_rs, sum_ss, sum_rs),
+    )
+    back_send[...] = expert_rows.astype(BF).reshape(n_sp, slots, columns)
+    to_sp(back_send, back_recv, back_ss, back_rs).wait_recv()
     returned = back_recv[...].reshape(count, columns)
     routed = dot(weight_high[...], returned) + dot(weight_low[...], returned)
-    last_send[...] = routed.astype(BF).reshape(n_tp, rows, columns)
-    last_all = to_tp(last_send, last_recv, last_ss, last_rs)
-    pending.append(last_all.wait_send)
-    last_all.wait_recv()
+    result = (mid_s[...] + routed).astype(BF)
+    last_send[...] = result.reshape(n_tp, rows, columns)
+    to_tp(last_send, last_recv, last_ss, last_rs).wait_recv()
     for j in range(n_tp):
-        lanes = slice(j * columns, (j + 1) * columns)
-        out[:, lanes] = (mid_s[:, lanes] + last_recv[j].astype(F32)).astype(BF)
+        out[:, j * columns : (j + 1) * columns] = last_recv[j]
 
     for finish in pending:
         finish()
@@ -682,7 +653,7 @@
     slots = 2 * length // n_sp
     count = n_sp * slots
     columns = width // n_tp
-    part = width // PARTS
+    pieces = min(PIECES, n_sp)
     own = hk // n_sp
     padded = (piece + 127) // 128 * 128
     vmem, any_space = (
@@ -705,25 +676,29 @@
         pltpu.VMEM((count, length), BF),
         pltpu.VMEM((length, count), BF),
         pltpu.VMEM((length, count), BF),
-        pltpu.VMEM((n_y, 2, rows, hv), BF),
-        pltpu.VMEM((PARTS, n_y, rows, part), BF),
-        pltpu.VMEM((PARTS, n_y, rows, part), BF),
-        pltpu.VMEM((PARTS, n_y, rows, part), F32),
-        pltpu.VMEM((2, half_ring, PARTS, rows, part), BF),
-        pltpu.VMEM((2, half_ring, PARTS, rows, part), BF),
-        pltpu.VMEM((rows, width), F32),
+        pltpu.VMEM((length, hv), BF),
         pltpu.VMEM((n_tp, rows, columns), BF),
         pltpu.VMEM((n_tp, rows, columns), BF),
+        pltpu.VMEM((n_y, pieces, length // pieces, columns), BF),
+        pltpu.VMEM((n_y, pieces, length // pieces, columns), BF),
+        pltpu.VMEM((n_y, pieces, length // pieces, columns), F32),
+        pltpu.VMEM((2, half_ring, pieces, length // pieces, columns), BF),
+        pltpu.VMEM((2, half_ring, pieces, length // pieces, columns), BF),
+        pltpu.VMEM((length, columns), F32),
+        pltpu.VMEM((n_tp, 1, length), F32),
+        pltpu.VMEM((n_tp, 1, length), F32),
+        pltpu.VMEM((n_sp, slots, BLK), BF),
+        pltpu.VMEM((n_sp, slots, BLK), BF),
         pltpu.VMEM((n_sp, slots, columns), BF),
         pltpu.VMEM((n_y, 2, n_sp, slots, columns), BF),
         pltpu.VMEM((count, piece), F32),
         pltpu.VMEM((count, piece), F32),
         pltpu.VMEM((count, padded), BF),
-        pltpu.VMEM((n_y, 2, count // 2, columns), BF),
-        pltpu.VMEM((n_y, 2, count // 2, columns), BF),
-        pltpu.VMEM((n_y, 2, count // 2, columns), F32),
-        pltpu.VMEM((2, half_ring, 2, count // 2, columns), BF),
-        pltpu.VMEM((2, half_ring, 2, count // 2, columns), BF),
+        pltpu.VMEM((n_y, pieces, count // pieces, columns), BF),
+        pltpu.VMEM((n_y, pieces, count // pieces, columns), BF),
+        pltpu.VMEM((n_y, pieces, count // pieces, columns), F32),
+        pltpu.VMEM((2, half_ring, pieces, count // pieces, columns), BF),
+        pltpu.VMEM((2, half_ring, pieces, count // pieces, columns), BF),
         pltpu.VMEM((n_sp, slots, columns), BF),
         pltpu.VMEM((n_sp, slots, columns), BF),
         pltpu.VMEM((n_tp, rows, columns), BF),
@@ -733,22 +708,26 @@
         dma((n_sp,)),
         dma,
         dma,
-        dma((PARTS,)),
-        dma((PARTS,)),
-        dma((2, half_ring, PARTS)),
-        dma((2, half_ring, PARTS)),
-        dma,
-        dma,
-        dma,
-        dma((n_sp,)),
-        dma((2, half_ring + 2, 2)),
-        dma((2, half_ring + 2, 2)),
-        dma((n_y, 2)),
-        dma((n_y, 2)),
+        dma,
+        dma,
         dma((n_y,)),
         dma((n_y,)),
-        dma((2, half_ring, 2)),
-        dma((2, half_ring, 2)),
+        dma((2, half_ring, pieces)),
+        dma((2, half_ring, pieces)),
+        dma,
+        dma,
+        dma,
+        dma,
+        dma,
+        dma((n_sp,)),
+        dma((2, half_ring + 2, pieces)),
+        dma((2, half_ring + 2, pieces)),
+        dma((n_y, pieces)),
+        dma((n_y, pieces)),
+        dma((n_y,)),
+        dma((n_y,)),
+        dma((2, half_ring, pieces)),
+        dma((2, half_ring, pieces)),
         dma,
         dma,
         dma,

time: 117 us -> 108 us (0.923)
  Pallas kernels: 115 us -> 106 us
    pallas_call x1, Pallas kernels: 115 us -> 106 us  [layer(): pl.pallas_call(functools.partial(layer_kernel, (n_sp, n_tp, rows, width,...]
where the time goes in v3:
time: 108 us
  Pallas kernels  106 us (98%)
  local copies, waits for them, and re-layouts  1.47 us (1%)
    pallas_call x1, Pallas kernels, layer(): pl.pallas_call(functools.partial(layer_kernel, (n_sp, n_tp, rows, width,...  106 us

profile of v3, /device:TPU:1, one launch (start us, length us, event | category | flops | bytes accessed | tf_op | source)
XLA Modules:
  0.0 107.7 jit_solution(2228800186448964291)
XLA Ops:
  0.0 106.2 %layer.1 = bf16[16,2048]{1,0:T(8,128)(2,1)} custom-call(bf16[16,2048]{1,0:T(8,128)(2,1)} %stream.1, bf16[256,256]{1,0:T(8,128)(2,1)} %queries.1, bf16[256,256]{1,0:T(8,128)(2,1)} %key_rows.1, bf16[256,512]{1,0:T(8,128)(2,1)} %values.1, bf16[16,256]{1,0:T(8,128)(2,1)} %bitcast.11, bf16[16,256]{1,0:T(8,128)(2,1)} %decay_matrix.1, f32[1,256]{1,0:T(1,128)} %bitcast.16, ...), custom_call_target="tpu_custom_call" | custom-call | tf_op jit(solution)/shard_map/layer/pallas_call | solution.py:736
  106.2 1.5 %copy.18 = bf16[16,2048]{1,0:T(8,128)(2,1)} copy(bf16[16,2048]{1,0:T(8,128)(2,1)} %layer.1) | data formatting | bytes 131072
